TPU v7x, 512 devices: a whole 4x4x16 slice. The times are simulated.
512 devices in a mesh: row: 64 (over z, y), col: 8 (over x, core).
Axes of the slice: x: 4, y: 4, z: 16, core: 2. Of those that a mesh axis runs over, the one named last changes fastest.
Arguments:
- tokens: bfloat16 [8, 12288, 2048], P('col', 'row'), may hold values from -6 to 6
- proj_in: bfloat16 [2048, 512], P('col'), may hold values from -0.125 to 0.125
- proj_out: bfloat16 [512, 2048], P(None, 'row'), may hold values from -0.25 to 0.25
Outputs:
- output: bfloat16 [8, 12288, 2048], P('col', 'row')
All inputs are finite; a program needn't handle non-finite values.
Results may differ from a plain program's by a relative error of at most 0.0083.
Values may be sent and summed in bfloat16 or wider, within the bound.
A program may use at most 64 MiB of HBM per device.

v0:
```python
import math

import jax
import jax.numpy as jnp
from jax import lax
from jax.sharding import Mesh
from jax.sharding import PartitionSpec as P

GRP = 128
ROW = ("row_0", "row_1")


highest = lax.Precision.HIGHEST
span_inner = 128


def copy_for_each(array, axis):
    copies = jnp.broadcast_to(array, (lax.axis_size(axis), *array.shape))
    return lax.all_to_all(copies, axis, split_axis=0, concat_axis=0, tiled=True)


def joined_along(tiles, dim):
    lengths = list(tiles.shape[1:])
    lengths[dim] *= tiles.shape[0]
    return jnp.moveaxis(tiles, 0, dim).reshape(lengths)


def gathered_copies(array, axis, dim):
    tiles = copy_for_each(array, axis)
    return joined_along(tiles, dim)


def in_blocks(array, dim, count):
    before, after = (array.shape[:dim], array.shape[dim + 1 :])
    return jnp.moveaxis(array.reshape(*before, count, -1, *after), dim, 0)


def turned_blocks(tiles, axes, sequence):
    inside = tiles.shape[1:]
    result = tiles.reshape(*(lax.axis_size(a) for a in axes), *inside)
    for k in sequence:
        result = lax.all_to_all(result, axes[k], k, k, tiled=True)
    return result.reshape(-1, *inside)


def exchange_by_axis(array, axes, sequence, split_dim, concat_dim):
    tiles = in_blocks(array, split_dim, lax.axis_size(axes))
    return joined_along(turned_blocks(tiles, axes, sequence), concat_dim)


def circle(height, breadth, period):
    product = lax.iota(jnp.int32, height)[:, None] * lax.iota(jnp.int32, breadth)[None, :] % period
    angle = product.astype(jnp.float32) * (2.0 * math.pi / period)
    return (jnp.cos(angle), jnp.sin(angle))


def mirror(values):
    return jnp.concatenate([values[:, :1], jnp.flip(values[:, 1:], 1)], 1)


def positions(piece):
    real_in = piece[0, 0]
    imag_in = piece[1, 0]
    count, length = real_in.shape
    outer = length // span_inner
    real_in = real_in.reshape(count, outer, span_inner)
    imag_in = imag_in.reshape(count, outer, span_inner)
    cos_one, sin_one = circle(outer, outer, outer)
    first_re = jnp.einsum("ab,kbq->kaq", cos_one, real_in, precision=highest) - jnp.einsum(
        "ab,kbq->kaq", sin_one, imag_in, precision=highest
    )
    first_im = jnp.einsum("ab,kbq->kaq", sin_one, real_in, precision=highest) + jnp.einsum(
        "ab,kbq->kaq", cos_one, imag_in, precision=highest
    )
    twist_c, twist_s = circle(outer, span_inner, length)
    turned_re = first_re * twist_c - first_im * twist_s
    turned_im = first_re * twist_s + first_im * twist_c
    cos_two, sin_two = circle(span_inner, span_inner, span_inner)
    factor = 1.0 / math.sqrt(GRP * length)
    real_out = jnp.einsum("kaq,qb->kba", turned_re, cos_two, precision=highest) - jnp.einsum(
        "kaq,qb->kba", turned_im, sin_two, precision=highest
    )
    real_out = real_out.reshape(count, length) * factor
    imag_out = jnp.einsum("kaq,qb->kba", turned_re, sin_two, precision=highest) + jnp.einsum(
        "kaq,qb->kba", turned_im, cos_two, precision=highest
    )
    imag_out = imag_out.reshape(count, length) * factor
    return jnp.stack([real_out, imag_out], 1)


def shards(tokens, proj_in, proj_out):
    seq_rows = tokens[0]
    local_len = seq_rows.shape[0]
    features = proj_in.shape[1]
    groups = features // GRP
    mapped = jnp.dot(
        seq_rows, gathered_copies(proj_in, "col", 0), preferred_element_type=jnp.float32
    ).astype(jnp.bfloat16)
    values = mapped.astype(jnp.float32).reshape(local_len, groups, GRP)
    cos_c, sin_c = circle(GRP, GRP, GRP)
    half = GRP // 2
    real_table = cos_c[:, :half]
    imag_table = jnp.concatenate([cos_c[:, half : half + 1], sin_c[:, 1:half]], 1)
    real_part = jnp.einsum("pgc,cs->gsp", values, real_table, precision=highest)
    imag_part = jnp.einsum("pgc,cs->gsp", values, imag_table, precision=highest)
    ways = lax.axis_size(ROW)
    slots = groups * real_table.shape[1]
    per_dev = slots // ways
    stacked = jnp.stack(
        [real_part.reshape(ways, per_dev, local_len), imag_part.reshape(ways, per_dev, local_len)],
        0,
    )
    spectra = positions(
        lax.all_to_all(
            stacked.astype(jnp.bfloat16), ROW, split_axis=1, concat_axis=3, tiled=True
        ).astype(stacked.dtype)
    )
    slot_ids = lax.axis_index(ROW) * per_dev + lax.iota(jnp.int32, per_dev)
    special = (slot_ids % half == 0)[:, None]
    real_g = spectra[:, 0]
    imag_g = spectra[:, 1]
    lower = jnp.where(special, 0.5 * (real_g + mirror(real_g)), real_g)
    upper = jnp.where(special, 0.5 * (imag_g + mirror(imag_g)), mirror(real_g))
    outgoing = jnp.stack([lower, upper], 1).astype(jnp.bfloat16)
    back = exchange_by_axis(outgoing, ROW, (0, 1), 2, 0)
    paired = back.reshape(groups, half, 2, local_len)
    low_half = paired[:, :, 0]
    high_half = paired[:, :, 1]
    mixed = jnp.concatenate([low_half, high_half[:, :1], jnp.flip(high_half[:, 1:], 1)], 1).reshape(
        features, local_len
    )
    result = lax.dot_general(
        mixed,
        lax.all_gather(proj_out, ROW, axis=1, tiled=True),
        (((0,), (0,)), ((), ())),
        preferred_element_type=jnp.float32,
    )
    return result.astype(jnp.bfloat16)[None]


def solution(mesh):
    split = Mesh(mesh.devices.reshape(16, 4, mesh.shape["col"]), ("row_0", "row_1", "col"))
    return jax.shard_map(
        shards,
        mesh=split,
        in_specs=(P("col", ROW, None), P("col", None), P(None, ROW)),
        out_specs=P("col", ROW, None),
        check_vma=False,
    )
```

profile of v0, /device:TPU:2, one launch (start us, length us, event | category | flops | bytes accessed | tf_op | source)
XLA Modules:
  0.0 218.3 jit_solution(16846580736775457972)
XLA Ops:
  6.5 2.5 %broadcast_in_dim.13 = bf16[8,256,512]{2,1,0:T(8,128)(2,1)} broadcast(bf16[256,512]{1,0:T(8,128)(2,1)} %param.4), dimensions={1,2} | broadcast | bytes 2359296 | tf_op jit(solution)/shard_map/broadcast_in_dim | solution.py:18
  9.1 9.4 %all-to-all-start = ((bf16[8,256,512]{2,1,0:T(8,128)(2,1)}), bf16[8,256,512]{2,1,0:T(8,128)(2,1)S(1)}, u32[]{:S(2)}, u32[]{:S(2)}) async-start(bf16[8,256,512]{2,1,0:T(8,128)(2,1)} %broadcast_in_dim.13), calls=%async_computation | async-start | bytes 4194304 | tf_op jit(solution)/shard_map/all_to_all | solution.py:19
  18.5 0.3 fusion.54
  18.7 0.3 fusion.53
  19.0 25.2 %all-to-all-done = bf16[8,256,512]{2,1,0:T(8,128)(2,1)S(1)} async-done(((bf16[8,256,512]{2,1,0:T(8,128)(2,1)}), bf16[8,256,512]{2,1,0:T(8,128)(2,1)S(1)}, u32[]{:S(2)}, u32[]{:S(2)}) %all-to-all-start) | async-done | bytes 2097184 | tf_op jit(solution)/shard_map/all_to_all | solution.py:19
  44.2 0.6 fusion.1
  44.8 0.5 fusion.8
  45.3 0.5 fusion.9
  45.9 0.9 pad_maximum_fusion
  46.8 14.1 %all-to-all-start.1 = ((bf16[2,64,4,192]{3,2,0,1:T(4,128)(2,1)}), bf16[2,64,4,192]{3,2,0,1:T(4,128)(2,1)S(1)}, u32[]{:S(2)}, u32[]{:S(2)}) async-start(bf16[2,64,4,192]{3,2,0,1:T(4,128)(2,1)} %pad_maximum_fusion), calls=%async_computation.1 | async-start | bytes 524288 | tf_op jit(solution)/shard_map/all_to_all | solution.py:114
  61.0 0.7 all-gather.2.cloned.1.call-update
  61.7 0.2 fusion.39
  61.9 21.3 %all-to-all-done.1 = bf16[2,64,4,192]{3,2,0,1:T(4,128)(2,1)S(1)} async-done(((bf16[2,64,4,192]{3,2,0,1:T(4,128)(2,1)}), bf16[2,64,4,192]{3,2,0,1:T(4,128)(2,1)S(1)}, u32[]{:S(2)}, u32[]{:S(2)}) %all-to-all-start.1) | async-done | bytes 196640 | tf_op jit(solution)/shard_map/all_to_all | solution.py:114
  83.6 0.4 fusion.35
  84.0 0.4 fusion.31
  84.6 0.4 fusion.6
  85.0 0.4 fusion.7
  85.4 0.6 fusion.22
  86.0 0.6 fusion.5
  86.7 0.2 mul.299
  87.3 0.6 fusion.18
  87.8 0.6 fusion.3
  88.6 0.2 mul.304
  88.9 8.4 %reverse = f32[4,12288]{1,0:T(4,128)S(1)} reverse(f32[4,12288]{1,0:T(4,128)S(1)} %bitcast.99), dimensions={1} | reverse | bytes 393216
  97.6 8.4 %reverse.1 = f32[4,12288]{1,0:T(4,128)S(1)} reverse(f32[4,12288]{1,0:T(4,128)S(1)} %bitcast.100), dimensions={1} | reverse | bytes 393216
  107.1 0.3 copy.87
  107.3 20.6 %all_to_all.30 = bf16[16,4,4,2,192]{4,3,2,1,0:T(2,128)(2,1)S(1)} all-to-all(bf16[16,4,4,2,192]{4,3,2,1,0:T(2,128)(2,1)S(1)} %bitcast.98), channel_id=1, replica_groups=mesh['row_0'=16,'row_1'=4,'col'=8] {'row_0'}, dimensions={0} | all-to-all | bytes 393216 | tf_op jit(solution)/shard_map/all_to_all | solution.py:42
  128.2 9.7 %all_to_all.31 = bf16[16,4,4,2,192]{4,3,2,0,1:T(2,128)(2,1)S(1)} all-to-all(bf16[16,4,4,2,192]{4,3,2,0,1:T(2,128)(2,1)S(1)} %copy.77), channel_id=1, replica_groups=mesh['row_0'=16,'row_1'=4,'col'=8] {'row_1'}, dimensions={1} | all-to-all | bytes 393216 | tf_op jit(solution)/shard_map/all_to_all | solution.py:42
  137.8 0.2 copy.78
  138.1 0.4 fusion.102
  138.8 69.3 %all-gather.2.cloned.1.call-done = bf16[512,2048]{0,1:T(8,128)(2,1)} async-done(((bf16[512,32]{0,1:T(8,128)(2,1)}), bf16[512,2048]{0,1:T(8,128)(2,1)}) %all-gather.2.cloned.1.call-update) | async-done | bytes 2097168 | tf_op jit(solution)/shard_map/all_gather | solution.py:134
  208.1 3.3 %fusion = bf16[1,192,2048]{2,1,0:T(8,128)(2,1)} fusion(bf16[512,192]{1,0:T(8,128)(2,1)S(1)} %bitcast.96, bf16[512,2048]{0,1:T(8,128)(2,1)} %all-gather.2.cloned.1.call-done), kind=kOutput, calls=%fused_computation.1 | convolution fusion | flops 403046400 | bytes 3080192 | tf_op jit(solution)/shard_map/dot_general | solution.py:132
  (37 shorter events, 3.2 us)
Async XLA Ops:
  6.5 37.7 %copy-start = (bf16[1,192,2048]{2,1,0:T(8,128)(2,1)S(1)}, bf16[1,192,2048]{2,1,0:T(8,128)(2,1)}, u32[]{:S(2)}) copy-start(bf16[1,192,2048]{2,1,0:T(8,128)(2,1)} %param.3) | copy-start | bytes 2359300
  9.1 35.1 %all-to-all-start = ((bf16[8,256,512]{2,1,0:T(8,128)(2,1)}), bf16[8,256,512]{2,1,0:T(8,128)(2,1)S(1)}, u32[]{:S(2)}, u32[]{:S(2)}) async-start(bf16[8,256,512]{2,1,0:T(8,128)(2,1)} %broadcast_in_dim.13), calls=%async_computation | async-start | bytes 4194304 | tf_op jit(solution)/shard_map/all_to_all | solution.py:19
  46.8 36.5 %all-to-all-start.1 = ((bf16[2,64,4,192]{3,2,0,1:T(4,128)(2,1)}), bf16[2,64,4,192]{3,2,0,1:T(4,128)(2,1)S(1)}, u32[]{:S(2)}, u32[]{:S(2)}) async-start(bf16[2,64,4,192]{3,2,0,1:T(4,128)(2,1)} %pad_maximum_fusion), calls=%async_computation.1 | async-start | bytes 524288 | tf_op jit(solution)/shard_map/all_to_all | solution.py:114
  60.9 147.2 %all-gather.2.cloned.1.call-start = ((), (), s32[]{:S(2)}) async-start(), calls=%async_computation.4 | async-start | bytes 2129920 | tf_op jit(solution)/shard_map/all_gather | solution.py:134
Sparse Core Ops, SparseCore 0:
  64.7 143.3 all-gather.1
where the time goes:
time: 219 us; the launch traced here: 218 us
  waiting for transfers between devices  116 us (53%)
  blocking collectives  30.3 us (14%)
  starting transfers between devices  23.6 us (11%)
  local copies, waits for them, and re-layouts  23.1 us (11%)
  between operations  13.7 us (6%)
  matrix products  8.83 us (4%)
  other arithmetic  2.26 us (1%)
    all_gather x1, waiting for transfers between devices, shards(): lax.all_gather(proj_out, ROW, axis=1, tiled=True)  69.3 us
    all_to_all x2, blocking collectives, turned_blocks(): result = lax.all_to_all(result, axes[k], k, k, tiled=True)  30.3 us
    all_to_all x1, waiting for transfers between devices, copy_for_each(): return lax.all_to_all(copies, axis, split_axis=0, concat_axis=0, tiled=True)  25.2 us
    all_to_all x1, waiting for transfers between devices, shards(): lax.all_to_all(stacked.astype(jnp.bfloat16), ROW, split_axis=1, concat_ax...  21.3 us
    unnamed x6, local copies, waits for them, and re-layouts  16.8 us
    all_to_all x1, starting transfers between devices, shards(): lax.all_to_all(stacked.astype(jnp.bfloat16), ROW, split_axis=1, concat_ax...  14.1 us
    all_to_all x1, starting transfers between devices, copy_for_each(): return lax.all_to_all(copies, axis, split_axis=0, concat_axis=0, tiled=True)  9.39 us
  transfers between devices with their start and end apart: 3, of which 3 were waited for; matrix products, arithmetic and copies ran while one was open for 12% of the time, Pallas kernels for 0%

commit v1 on v0

v1 whole, which is shorter than its diff:
```python
import math

import jax
import jax.numpy as jnp
import numpy as np
from jax import lax
from jax.experimental import pallas as pl
from jax.experimental.pallas import tpu as pltpu
from jax.sharding import PartitionSpec as P

MESH = pl.DeviceIdType.MESH
GRP = 128
GROUPS = 4
NZ, NY, NX = 16, 4, 4
ROWS = NZ * NY
LOC = 192
LEN = ROWS * LOC
D = 2048
KS = 256
FW = GROUPS * GRP
F32 = jnp.float32
BF = jnp.bfloat16


def tables():
    s = np.arange(64)[:, None]
    f = np.arange(GRP)[None, :]
    ang = 2 * np.pi * ((s * f) % GRP) / GRP
    part_a = np.cos(ang)
    part_b = np.sin(ang)
    part_b[0] = np.cos(np.pi * np.arange(GRP))
    chan = np.concatenate([part_a, part_b], 1)
    q = np.arange(LOC)[:, None]
    p1 = np.arange(LOC)[None, :]
    ang = 2 * np.pi * ((q * p1) % LOC) / LOC
    first = np.repeat(np.concatenate([np.cos(ang), np.sin(ang)], 0), 4, axis=1)
    q2 = np.arange(64)[None, :]
    ang = 2 * np.pi * ((q * q2) % LEN) / LEN
    scale = 1.0 / math.sqrt(GRP * LEN)
    twist = np.stack([np.tile(np.cos(ang), (1, 2)), np.tile(np.sin(ang), (1, 2))]) * scale
    r = np.arange(64)[:, None]
    ang = 2 * np.pi * ((r * q2) % 64) / 64
    c, n = np.cos(ang), np.sin(ang)
    last = np.repeat(np.concatenate([c, n, -n, c], 1), 4, axis=0)
    return chan, first, twist, last


def bdot(a, b):
    return lax.dot_general(a, b, (((1,), (1,)), ((), ())), preferred_element_type=F32)


def kernel(tok_hbm, win_hbm, pout_hbm, chan_hbm, first_hbm, twist_hbm, last_hbm, out_ref, tok, wfull, pblk, chan, first, twist, last, m1, l3, blk, pt, snd, dat, snd2, dat2, pgx, ld, pin_s, pin_r, a1_s, a1_r, a2_s, a2_r, pz_s, pz_r, py_s, py_r, px_s, px_r):
    row = lax.axis_index("row")
    col = lax.axis_index("col")
    z, y = row // NY, lax.rem(row, NY)
    x, core = col // 2, lax.rem(col, 2)
    xr = lax.rem(x + 1, NX)
    xl = lax.rem(x + NX - 1, NX)
    xo = lax.rem(x + 2, NX)
    right, left, mate = xr * 2 + core, xl * 2 + core, x * 2 + (1 - core)

    bar = pltpu.get_barrier_semaphore()

    def greet_row(o, c):
        pl.semaphore_signal(bar, inc=1, device_id={"row": lax.rem(row + o, ROWS)}, device_id_type=MESH)
        return c

    lax.fori_loop(1, ROWS, greet_row, 0)
    for peer in (right, left, mate):
        pl.semaphore_signal(bar, inc=1, device_id={"col": peer}, device_id_type=MESH)

    loads = [
        pltpu.make_async_copy(win_hbm, wfull.at[pl.ds(pl.multiple_of(col * KS, KS), KS), :], ld.at[0]),
        pltpu.make_async_copy(pout_hbm, pblk, ld.at[1]),
        pltpu.make_async_copy(tok_hbm.at[0], tok, ld.at[2]),
        pltpu.make_async_copy(chan_hbm, chan, ld.at[3]),
        pltpu.make_async_copy(first_hbm, first, ld.at[4]),
        pltpu.make_async_copy(last_hbm, last, ld.at[5]),
        pltpu.make_async_copy(twist_hbm, twist, ld.at[6]),
    ]
    for c in loads:
        c.start()

    rid = lax.broadcasted_iota(jnp.int32, (FW, FW), 1)
    fid = lax.broadcasted_iota(jnp.int32, (FW, FW), 0)
    inner = lax.rem(rid, 256)
    slot = (inner // 16) * 4 + lax.rem(inner, 4)
    upper = jnp.where(slot == 0, 64, GRP - slot)
    want = lax.rem(inner // 4, 4) * GRP + jnp.where(rid < 256, slot, upper)
    perm = jnp.where(fid == want, 1.0, 0.0).astype(BF)
    loads[1].wait()
    turned = lax.dot_general(pblk[...], perm, (((0,), (0,)), ((), ())), preferred_element_type=F32).astype(BF)
    blk[...] = turned

    for i in (3, 4, 5, 6):
        loads[i].wait()
    lane = lax.rem(lax.broadcasted_iota(jnp.int32, (2 * LOC, 4 * LOC), 1), 4)
    sub = lax.rem(lax.broadcasted_iota(jnp.int32, (256, 256), 0), 4)
    for s in range(4):
        m1[s] = first[...] * jnp.where(lane == s, 1.0, 0.0).astype(BF)
        l3[s] = last[...] * jnp.where(sub == s, 1.0, 0.0).astype(BF)
    loads[0].wait()
    loads[2].wait()

    pl.semaphore_wait(bar, ROWS - 1 + 3)

    def wtile(c, g, lo=0, n=KS):
        return wfull.at[pl.ds(pl.multiple_of(c * KS + lo, 128), n), pl.ds(pl.multiple_of(g * GRP, GRP), GRP)]

    def push(ref, ss, rs, peer):
        return pltpu.make_async_remote_copy(src_ref=ref, dst_ref=ref, send_sem=ss, recv_sem=rs, device_id={"col": peer}, device_id_type=MESH)

    def pin(t, k, g):
        who = (col, col, col, xl * 2 + core, xr * 2 + core, xl * 2 + core, xr * 2 + core, xo * 2 + core, xo * 2 + core)[k]
        lo = (0, 0, 0, 0, 128, 0, 0, 0, 128)[k]
        n = (KS, KS, KS, 128, 128, KS, KS, 128, 128)[k]
        peer = (right, left, mate, right, left, mate, mate, mate, mate)[k]
        return push(wtile(who, g, lo, n), pin_s.at[t, k], pin_r.at[t, k], peer)

    def pin_arrived(t, k, g):
        n = (KS, KS, KS, 128, 128, KS, KS, 128, 128)[k]
        push(wtile(col, g, 0, n), pin_s.at[t, k], pin_r.at[t, k], mate).wait_recv()

    gs = [lax.rem(y + t, GROUPS) for t in range(GROUPS)]
    for t in range(GROUPS):
        for k in range(3):
            pin(t, k, gs[t]).start()

    half = pl.ds(pl.multiple_of(core * 16, 16), 16)
    quarter = pl.ds(pl.multiple_of(x * GRP, GRP), GRP)
    own = pltpu.make_async_copy(blk.at[half, quarter], pgx.at[row], ld.at[7])
    own.start()

    def pz_send(o, c):
        to = lax.rem(row + NY * o, ROWS)
        pltpu.make_async_remote_copy(src_ref=blk.at[half, quarter], dst_ref=pgx.at[row], send_sem=pz_s, recv_sem=pz_r, device_id={"row": to}, device_id_type=MESH).start()
        return c

    own.wait()

    for t in range(GROUPS):
        g = gs[t]
        pin_arrived(t, 0, g)
        pin(t, 3, g).start()
        pin(t, 5, g).start()
        pin_arrived(t, 1, g)
        pin(t, 4, g).start()
        pin(t, 6, g).start()
        pin_arrived(t, 3, g)
        pin(t, 7, g).start()
        pin_arrived(t, 4, g)
        pin(t, 8, g).start()
        for k in (2, 5, 6, 7, 8):
            pin_arrived(t, k, g)
        w = wfull[:, pl.ds(pl.multiple_of(g * GRP, GRP), GRP)]
        mapped = jnp.dot(tok[...], w, preferred_element_type=F32).astype(BF)
        zero = jnp.zeros((64, GRP), BF)
        parts = []
        for m in range(3):
            piece = mapped[64 * m : 64 * m + 64]
            parts.append(jnp.concatenate([piece, zero], 1))
            parts.append(jnp.concatenate([zero, piece], 1))
        spread = bdot(chan[...], jnp.concatenate(parts, 0))
        for m in range(3):
            snd[t, :, m] = spread[:, GRP * m : GRP * m + GRP].reshape(NZ, 4, GRP).astype(BF)

        def a1_send(o, c, t=t, g=g):
            to = lax.rem(z + o, NZ)
            pltpu.make_async_remote_copy(src_ref=snd.at[t, to], dst_ref=dat.at[row], send_sem=a1_s.at[t], recv_sem=a1_r, device_id={"row": to * NY + g}, device_id_type=MESH).start()
            return c

        if t == 0:
            pltpu.make_async_copy(snd.at[0, z], dat.at[row], a1_r).start()
            lax.fori_loop(1, NZ, a1_send, 0)
        else:
            lax.fori_loop(0, NZ, a1_send, 0)

    lax.fori_loop(1, NZ, pz_send, 0)

    def zpart(yy):
        return pgx.at[pl.ds(0, NZ)]

    pltpu.make_async_copy(pgx.at[pl.ds(0, NZ - 1)], pgx.at[pl.ds(0, NZ - 1)], pz_r).wait()
    for o in range(1, NY):
        yo = lax.rem(y + o, NY)

        def py_send(k, c, yo=yo, o=o):
            pltpu.make_async_remote_copy(src_ref=pgx.at[k * NY + y], dst_ref=pgx.at[k * NY + y], send_sem=py_s.at[o - 1], recv_sem=py_r, device_id={"row": z * NY + yo}, device_id_type=MESH).start()
            return c

        lax.fori_loop(0, NZ, py_send, 0)

    pltpu.make_async_copy(dat, dat, a1_r).wait()
    data = dat[...].reshape(4 * LOC, GRP)
    cc, sn = twist[0], twist[1]
    first_slot = z == 0
    lanes = lax.broadcasted_iota(jnp.int32, (1, GRP), 1) < 64
    sgn = jnp.where(lanes, 1.0, -1.0)
    zero_b = jnp.where(lanes, 1.0, 0.0)
    spec = jnp.where(first_slot, 1.0, 0.0)
    outs = [None] * 3
    for s in range(4):
        got = jnp.dot(m1[s], data, preferred_element_type=F32)
        re, im = got[:LOC], got[LOC:]
        tre = re * cc - im * sn
        tim = re * sn + im * cc
        if s == 0:
            lo_mask = zero_b * spec + sgn * (1.0 - spec)
            up_keep, up_turn = 1.0 - spec, zero_b * spec
            lo_re, lo_im = tre * lo_mask, tim * lo_mask
            up_re = tre * up_keep + pltpu.roll(tre, 64, 1) * up_turn
            up_im = tim * up_keep + pltpu.roll(tim, 64, 1) * up_turn
        else:
            lo_re, lo_im, up_re, up_im = tre * sgn, tim * sgn, tre, tim
        lo = jnp.concatenate([lo_re, lo_im], 1).astype(BF)
        up = jnp.concatenate([up_re, up_im], 1).astype(BF)
        for m in range(3):
            rhs = jnp.concatenate([lo[64 * m : 64 * m + 64], up[64 * m : 64 * m + 64]], 0)
            term = bdot(l3[s], rhs)
            outs[m] = term if outs[m] is None else outs[m] + term
    for m in range(3):
        snd2[:, m] = outs[m].reshape(ROWS, 4, GRP).astype(BF)

    pltpu.make_async_copy(snd2.at[row], dat2.at[row], a2_r).start()

    def a2_send(o, c):
        to = lax.rem(row + o, ROWS)
        pltpu.make_async_remote_copy(src_ref=snd2.at[to], dst_ref=dat2.at[row], send_sem=a2_s, recv_sem=a2_r, device_id={"row": to}, device_id_type=MESH).start()
        return c

    lax.fori_loop(1, ROWS, a2_send, 0)

    pltpu.make_async_copy(pgx.at[pl.ds(0, 3 * NZ)], pgx.at[pl.ds(0, 3 * NZ)], py_r).wait()

    def ptile(c, lo=0, n=ROWS):
        return pt.at[pl.ds(lo, n), pl.ds(pl.multiple_of(lax.rem(c, 2) * 16, 16), 16), pl.ds(pl.multiple_of((c // 2) * GRP, GRP), GRP)]

    mine = pltpu.make_async_copy(pgx, ptile(col), ld.at[8])
    mine.start()
    mine.wait()

    def px(k):
        who = (col, col, col, xl * 2 + core, xr * 2 + core, xl * 2 + core, xr * 2 + core, xo * 2 + core, xo * 2 + core)[k]
        lo = (0, 0, 0, 0, 32, 0, 0, 0, 32)[k]
        n = (64, 64, 64, 32, 32, 64, 64, 32, 32)[k]
        peer = (right, left, mate, right, left, mate, mate, mate, mate)[k]
        return push(ptile(who, lo, n), px_s.at[k], px_r.at[k], peer)

    def px_arrived(k):
        n = (64, 64, 64, 32, 32, 64, 64, 32, 32)[k]
        push(ptile(col, 0, n), px_s.at[k], px_r.at[k], mate).wait_recv()

    for k in range(3):
        px(k).start()
    px_arrived(0)
    px(3).start()
    px(5).start()
    px_arrived(1)
    px(4).start()
    px(6).start()
    px_arrived(3)
    px(7).start()
    px_arrived(4)
    px(8).start()
    for k in (2, 5, 6, 7, 8):
        px_arrived(k)

    pltpu.make_async_copy(dat2, dat2, a2_r).wait()
    sides = []
    for m in range(3):
        t = dat2[:, m].reshape(256, GRP).T
        sides.append(jnp.concatenate([t[:64], t[64:]], 1))
    lhs = jnp.concatenate(sides, 0)
    for n in range(8):
        out_ref[0, :, 256 * n : 256 * n + 256] = bdot(lhs, pt[8 * n : 8 * n + 8].reshape(256, FW)).astype(BF)

    for t in range(GROUPS):
        for k in range(9):
            pin(t, k, gs[t]).wait_send()
        n = NZ - 1 if t == 0 else NZ
        pltpu.make_async_copy(snd.at[t, pl.ds(0, n)], snd.at[t, pl.ds(0, n)], a1_s.at[t]).wait()
    for k in range(9):
        px(k).wait_send()
    pltpu.make_async_copy(pgx.at[pl.ds(0, NZ - 1)], pgx.at[pl.ds(0, NZ - 1)], pz_s).wait()
    for o in range(3):
        pltpu.make_async_copy(pgx.at[pl.ds(0, NZ)], pgx.at[pl.ds(0, NZ)], py_s.at[o]).wait()
    pltpu.make_async_copy(snd2.at[pl.ds(0, ROWS - 1)], snd2.at[pl.ds(0, ROWS - 1)], a2_s).wait()


def shards(tokens, proj_in, proj_out):
    chan, first, twist, last = tables()
    anyspec = pl.BlockSpec(memory_space=pl.ANY)
    dma = pltpu.SemaphoreType.DMA
    return pl.pallas_call(
        kernel,
        out_shape=jax.ShapeDtypeStruct((1, LOC, D), BF),
        in_specs=[anyspec] * 7,
        out_specs=pl.BlockSpec(memory_space=pltpu.VMEM),
        scratch_shapes=[
            pltpu.VMEM((LOC, D), BF),
            pltpu.VMEM((D, FW), BF),
            pltpu.VMEM((FW, 32), BF),
            pltpu.VMEM((64, 256), BF),
            pltpu.VMEM((2 * LOC, 4 * LOC), BF),
            pltpu.VMEM((2, LOC, GRP), F32),
            pltpu.VMEM((256, 256), BF),
            pltpu.VMEM((4, 2 * LOC, 4 * LOC), BF),
            pltpu.VMEM((4, 256, 256), BF),
            pltpu.VMEM((32, FW), BF),
            pltpu.VMEM((ROWS, 32, FW), BF),
            pltpu.VMEM((GROUPS, NZ, 3, 4, GRP), BF),
            pltpu.VMEM((ROWS, 3, 4, GRP), BF),
            pltpu.VMEM((ROWS, 3, 4, GRP), BF),
            pltpu.VMEM((ROWS, 3, 4, GRP), BF),
            pltpu.VMEM((ROWS, 16, GRP), BF),
            dma((9,)),
            dma((GROUPS, 9)),
            dma((GROUPS, 9)),
            dma((GROUPS,)),
            dma,
            dma,
            dma,
            dma,
            dma,
            dma((3,)),
            dma,
            dma((9,)),
            dma((9,)),
        ],
        compiler_params=pltpu.CompilerParams(collective_id=0, has_side_effects=True),
    )(
        tokens,
        proj_in,
        proj_out,
        jnp.asarray(chan, BF),
        jnp.asarray(first, BF),
        jnp.asarray(twist, F32),
        jnp.asarray(last, BF),
    )


def solution(mesh):
    return jax.shard_map(
        shards,
        mesh=mesh,
        in_specs=(P("col", "row", None), P("col", None), P(None, "row")),
        out_specs=P("col", "row", None),
        check_vma=False,
    )
```

time: 219 us -> 77 us (0.35)
  the two profiles are of different devices: /device:TPU:2 before, /device:TPU:1 now
where the time goes in v1:
time: 77 us; the launch traced here: 76.8 us
  Pallas kernels  73.2 us (95%)
  local copies, waits for them, and re-layouts  3.61 us (5%)
    pallas_call x1, Pallas kernels, shards(): pl.pallas_call(kernel, out_shape=jax.ShapeDtypeStruct((1, LOC, D), BF), i...  73.2 us
    unnamed x2, local copies, waits for them, and re-layouts  3.61 us

profile of v1, /device:TPU:1, one launch (start us, length us, event | category | flops | bytes accessed | tf_op | source)
XLA Modules:
  0.0 76.8 jit_solution(8023527038128940973)
XLA Ops:
  0.0 1.5 %copy.8.pout_hbm = bf16[512,32]{1,0:T(8,128)(2,1)} copy(bf16[512,32]{0,1:T(8,128)(2,1)} %param.9) | data formatting | bytes 65536 | tf_op args[2]
  1.5 73.2 %shard_map.73 = bf16[1,192,2048]{2,1,0:T(8,128)(2,1)} custom-call(bf16[1,192,2048]{2,1,0:T(8,128)(2,1)} %tok_hbm.1, bf16[256,512]{1,0:T(8,128)(2,1)} %win_hbm.1, bf16[512,32]{1,0:T(8,128)(2,1)} %copy.8.pout_hbm, bf16[64,256]{1,0:T(8,128)(2,1)} %constant.8.clone.chan_hbm, bf16[384,768]{1,0:T(8,128)(2,1)} %constant.9.clone.first_hbm, ...), custom_call_target="tpu_custom_call" | custom-call | tf_op jit(solution)/shard_map/pallas_call | solution.py:294
  74.7 2.1 %copy.10 = bf16[1,192,2048]{2,1,0:T(8,128)(2,1)} copy(bf16[1,192,2048]{2,1,0:T(8,128)(2,1)} %shard_map.73) | data formatting | bytes 1572864

commit v2 on v1

--- a/solution.py
+++ b/solution.py
@@ -49,7 +49,7 @@
     return lax.dot_general(a, b, (((1,), (1,)), ((), ())), preferred_element_type=F32)
 
 
-def kernel(tok_hbm, win_hbm, pout_hbm, chan_hbm, first_hbm, twist_hbm, last_hbm, out_ref, tok, wfull, pblk, chan, first, twist, last, m1, l3, blk, pt, snd, dat, snd2, dat2, pgx, ld, pin_s, pin_r, a1_s, a1_r, a2_s, a2_r, pz_s, pz_r, py_s, py_r, px_s, px_r):
+def kernel(tok_hbm, win_hbm, pout_hbm, chan_hbm, first_hbm, twist_hbm, last_hbm, out_ref, tok, wfull, pblk, chan, first, twist, last, m1, l3, blk, pt, snd, dat, snd2, dat2, pgx, ld, hops, pin_s, pin_r, yin_s, yin_r, ymt_s, ymt_r, a1_s, a1_r, a2_s, a2_r, pz_s, pz_r, py_s, py_r, px_s, px_r):
     row = lax.axis_index("row")
     col = lax.axis_index("col")
     z, y = row // NY, lax.rem(row, NY)
@@ -58,16 +58,16 @@
     xl = lax.rem(x + NX - 1, NX)
     xo = lax.rem(x + 2, NX)
     right, left, mate = xr * 2 + core, xl * 2 + core, x * 2 + (1 - core)
+    yu, yd, yo = lax.rem(y + 1, NY), lax.rem(y + NY - 1, NY), lax.rem(y + 2, NY)
+
+    def at(dz, yy):
+        return lax.rem(z + dz, NZ) * NY + yy
 
     bar = pltpu.get_barrier_semaphore()
-
-    def greet_row(o, c):
-        pl.semaphore_signal(bar, inc=1, device_id={"row": lax.rem(row + o, ROWS)}, device_id_type=MESH)
-        return c
-
-    lax.fori_loop(1, ROWS, greet_row, 0)
     for peer in (right, left, mate):
         pl.semaphore_signal(bar, inc=1, device_id={"col": peer}, device_id_type=MESH)
+    for peer in (at(0, yu), at(0, yd), at(1, y), at(NZ - 1, y)):
+        pl.semaphore_signal(bar, inc=1, device_id={"row": peer}, device_id_type=MESH)
 
     loads = [
         pltpu.make_async_copy(win_hbm, wfull.at[pl.ds(pl.multiple_of(col * KS, KS), KS), :], ld.at[0]),
@@ -80,6 +80,68 @@
     ]
     for c in loads:
         c.start()
+    loads[0].wait()
+    pl.semaphore_wait(bar, 7)
+
+    same = [col, xl * 2 + core, xr * 2 + core, xo * 2 + core, xo * 2 + core]
+    begin = [0, 0, 0, 0, 128]
+    length = [KS, KS, KS, 128, 128]
+
+    def wtile(k, g):
+        return wfull.at[pl.ds(pl.multiple_of(same[k] * KS + begin[k], 128), length[k]), pl.ds(pl.multiple_of(g * GRP, GRP), GRP)]
+
+    def other(k, g):
+        return wfull.at[pl.ds(pl.multiple_of((same[k] + 1 - 2 * core) * KS + begin[k], 128), length[k]), pl.ds(pl.multiple_of(g * GRP, GRP), GRP)]
+
+    def push(ref, ss, rs, peer):
+        return pltpu.make_async_remote_copy(src_ref=ref, dst_ref=ref, send_sem=ss, recv_sem=rs, device_id=peer, device_id_type=MESH)
+
+    xg = (y, yo)
+    yg = (yu, yd)
+
+    def along_x(t, k):
+        piece = (0, 0, 3, 4)[k]
+        who = (None, None, xl * 2 + core, xr * 2 + core)[k]
+        ref = wtile(0, xg[t])
+        if k >= 2:
+            ref = wfull.at[pl.ds(pl.multiple_of(who * KS + begin[piece], 128), 128), pl.ds(pl.multiple_of(xg[t] * GRP, GRP), GRP)]
+        return push(ref, pin_s.at[t, k], pin_r.at[t, k], {"col": (right, left, right, left)[k]})
+
+    def x_arrived(t, k):
+        along_x(t, k).wait_recv()
+
+    def to_mate(t, k):
+        return push(wtile(k, (*xg, *yg)[t]), ymt_s.at[t, k], ymt_r.at[t, k], {"col": mate})
+
+    def from_mate(t, k):
+        push(other(k, (*xg, *yg)[t]), ymt_s.at[t, k], ymt_r.at[t, k], {"col": mate}).wait_recv()
+
+    def along_y(d, k):
+        return push(wtile(k, y), yin_s.at[d, k], yin_r.at[d, k], {"row": at(0, (yu, yd)[d])})
+
+    def y_arrived(d, k):
+        push(wtile(k, (yd, yu)[d]), yin_s.at[d, k], yin_r.at[d, k], {"row": at(0, (yu, yd)[d])}).wait_recv()
+
+    def piece_in(t, k):
+        to_mate(t, k).start()
+        if t == 0 and k > 0:
+            along_y(0, k).start()
+            along_y(1, k).start()
+
+    along_x(0, 0).start()
+    along_x(0, 1).start()
+    piece_in(0, 0)
+    along_x(1, 0).start()
+    along_x(1, 1).start()
+    piece_in(1, 0)
+    to_mate(2, 0).start()
+    to_mate(3, 0).start()
+
+    def tell(i, peers):
+        for peer in peers:
+            pl.semaphore_signal(hops.at[i], inc=1, device_id={"row": peer}, device_id_type=MESH)
+
+    tell(0, (at(1, y), at(NZ - 1, y), at(0, yu), at(0, yd)))
 
     rid = lax.broadcasted_iota(jnp.int32, (FW, FW), 1)
     fid = lax.broadcasted_iota(jnp.int32, (FW, FW), 0)
@@ -89,8 +151,10 @@
     want = lax.rem(inner // 4, 4) * GRP + jnp.where(rid < 256, slot, upper)
     perm = jnp.where(fid == want, 1.0, 0.0).astype(BF)
     loads[1].wait()
-    turned = lax.dot_general(pblk[...], perm, (((0,), (0,)), ((), ())), preferred_element_type=F32).astype(BF)
-    blk[...] = turned
+    blk[...] = jnp.dot(pblk[...], perm, preferred_element_type=F32).astype(BF)
+
+    pl.semaphore_wait(hops.at[0], 4)
+    tell(1, (at(2, y), at(NZ - 2, y)))
 
     for i in (3, 4, 5, 6):
         loads[i].wait()
@@ -99,59 +163,61 @@
     for s in range(4):
         m1[s] = first[...] * jnp.where(lane == s, 1.0, 0.0).astype(BF)
         l3[s] = last[...] * jnp.where(sub == s, 1.0, 0.0).astype(BF)
-    loads[0].wait()
+
+    pl.semaphore_wait(hops.at[1], 2)
+    tell(2, (at(4, y), at(NZ - 4, y)))
+
+    for t in range(2):
+        x_arrived(t, 0)
+        along_x(t, 2).start()
+        piece_in(t, 1)
+        x_arrived(t, 1)
+        along_x(t, 3).start()
+        piece_in(t, 2)
+
+    pl.semaphore_wait(hops.at[2], 2)
+    tell(3, (at(0, yu), at(0, yd), at(0, yo)))
+
+    for k in (3, 4):
+        x_arrived(0, k - 1)
+        piece_in(0, k)
+    for k in (3, 4):
+        x_arrived(1, k - 1)
+        piece_in(1, k)
+    for d in range(2):
+        for k in (1, 2):
+            y_arrived(d, k)
+            to_mate(3 - d, k).start()
     loads[2].wait()
 
-    pl.semaphore_wait(bar, ROWS - 1 + 3)
-
-    def wtile(c, g, lo=0, n=KS):
-        return wfull.at[pl.ds(pl.multiple_of(c * KS + lo, 128), n), pl.ds(pl.multiple_of(g * GRP, GRP), GRP)]
-
-    def push(ref, ss, rs, peer):
-        return pltpu.make_async_remote_copy(src_ref=ref, dst_ref=ref, send_sem=ss, recv_sem=rs, device_id={"col": peer}, device_id_type=MESH)
-
-    def pin(t, k, g):
-        who = (col, col, col, xl * 2 + core, xr * 2 + core, xl * 2 + core, xr * 2 + core, xo * 2 + core, xo * 2 + core)[k]
-        lo = (0, 0, 0, 0, 128, 0, 0, 0, 128)[k]
-        n = (KS, KS, KS, 128, 128, KS, KS, 128, 128)[k]
-        peer = (right, left, mate, right, left, mate, mate, mate, mate)[k]
-        return push(wtile(who, g, lo, n), pin_s.at[t, k], pin_r.at[t, k], peer)
-
-    def pin_arrived(t, k, g):
-        n = (KS, KS, KS, 128, 128, KS, KS, 128, 128)[k]
-        push(wtile(col, g, 0, n), pin_s.at[t, k], pin_r.at[t, k], mate).wait_recv()
-
-    gs = [lax.rem(y + t, GROUPS) for t in range(GROUPS)]
-    for t in range(GROUPS):
-        for k in range(3):
-            pin(t, k, gs[t]).start()
+    pl.semaphore_wait(hops.at[3], 3)
 
     half = pl.ds(pl.multiple_of(core * 16, 16), 16)
     quarter = pl.ds(pl.multiple_of(x * GRP, GRP), GRP)
     own = pltpu.make_async_copy(blk.at[half, quarter], pgx.at[row], ld.at[7])
     own.start()
 
-    def pz_send(o, c):
-        to = lax.rem(row + NY * o, ROWS)
-        pltpu.make_async_remote_copy(src_ref=blk.at[half, quarter], dst_ref=pgx.at[row], send_sem=pz_s, recv_sem=pz_r, device_id={"row": to}, device_id_type=MESH).start()
+    def far(i):
+        step = (i + 1) // 2
+        return lax.rem(8 + step * (1 - 2 * lax.rem(i, 2)) + NZ, NZ)
+
+    def pz_send(i, c):
+        pltpu.make_async_remote_copy(src_ref=blk.at[half, quarter], dst_ref=pgx.at[row], send_sem=pz_s, recv_sem=pz_r, device_id={"row": at(far(i), y)}, device_id_type=MESH).start()
         return c
 
+    lax.fori_loop(0, NZ - 1, pz_send, 0)
     own.wait()
 
+    order = (y, yo, yu, yd)
     for t in range(GROUPS):
-        g = gs[t]
-        pin_arrived(t, 0, g)
-        pin(t, 3, g).start()
-        pin(t, 5, g).start()
-        pin_arrived(t, 1, g)
-        pin(t, 4, g).start()
-        pin(t, 6, g).start()
-        pin_arrived(t, 3, g)
-        pin(t, 7, g).start()
-        pin_arrived(t, 4, g)
-        pin(t, 8, g).start()
-        for k in (2, 5, 6, 7, 8):
-            pin_arrived(t, k, g)
+        g = order[t]
+        if t == 2:
+            for d in range(2):
+                for k in (3, 4):
+                    y_arrived(d, k)
+                    to_mate(3 - d, k).start()
+        for k in range(5):
+            from_mate(t, k)
         w = wfull[:, pl.ds(pl.multiple_of(g * GRP, GRP), GRP)]
         mapped = jnp.dot(tok[...], w, preferred_element_type=F32).astype(BF)
         zero = jnp.zeros((64, GRP), BF)
@@ -164,31 +230,46 @@
         for m in range(3):
             snd[t, :, m] = spread[:, GRP * m : GRP * m + GRP].reshape(NZ, 4, GRP).astype(BF)
 
-        def a1_send(o, c, t=t, g=g):
-            to = lax.rem(z + o, NZ)
+        def a1_send(i, c, t=t, g=g):
+            to = lax.rem(z + far(i), NZ)
             pltpu.make_async_remote_copy(src_ref=snd.at[t, to], dst_ref=dat.at[row], send_sem=a1_s.at[t], recv_sem=a1_r, device_id={"row": to * NY + g}, device_id_type=MESH).start()
             return c
 
+        lax.fori_loop(0, NZ - 1 if t == 0 else NZ, a1_send, 0)
         if t == 0:
             pltpu.make_async_copy(snd.at[0, z], dat.at[row], a1_r).start()
-            lax.fori_loop(1, NZ, a1_send, 0)
-        else:
-            lax.fori_loop(0, NZ, a1_send, 0)
-
-    lax.fori_loop(1, NZ, pz_send, 0)
-
-    def zpart(yy):
-        return pgx.at[pl.ds(0, NZ)]
 
     pltpu.make_async_copy(pgx.at[pl.ds(0, NZ - 1)], pgx.at[pl.ds(0, NZ - 1)], pz_r).wait()
     for o in range(1, NY):
-        yo = lax.rem(y + o, NY)
-
-        def py_send(k, c, yo=yo, o=o):
-            pltpu.make_async_remote_copy(src_ref=pgx.at[k * NY + y], dst_ref=pgx.at[k * NY + y], send_sem=py_s.at[o - 1], recv_sem=py_r, device_id={"row": z * NY + yo}, device_id_type=MESH).start()
+
+        def py_send(k, c, o=o):
+            pltpu.make_async_remote_copy(src_ref=pgx.at[k * NY + y], dst_ref=pgx.at[k * NY + y], send_sem=py_s.at[o - 1], recv_sem=py_r, device_id={"row": at(0, lax.rem(y + o, NY))}, device_id_type=MESH).start()
             return c
 
         lax.fori_loop(0, NZ, py_send, 0)
+
+    pltpu.make_async_copy(pgx.at[pl.ds(0, 3 * NZ)], pgx.at[pl.ds(0, 3 * NZ)], py_r).wait()
+
+    def ptile(c, lo=0, n=ROWS):
+        return pt.at[pl.ds(lo, n), pl.ds(pl.multiple_of(lax.rem(c, 2) * 16, 16), 16), pl.ds(pl.multiple_of((c // 2) * GRP, GRP), GRP)]
+
+    mine = pltpu.make_async_copy(pgx, ptile(col), ld.at[8])
+    mine.start()
+    mine.wait()
+
+    def px(k):
+        who = (col, col, col, xl * 2 + core, xr * 2 + core, xl * 2 + core, xr * 2 + core, xo * 2 + core, xo * 2 + core)[k]
+        lo = (0, 0, 0, 0, 32, 0, 0, 0, 32)[k]
+        n = (64, 64, 64, 32, 32, 64, 64, 32, 32)[k]
+        peer = (right, left, mate, right, left, mate, mate, mate, mate)[k]
+        return push(ptile(who, lo, n), px_s.at[k], px_r.at[k], {"col": peer})
+
+    def px_arrived(k):
+        n = (64, 64, 64, 32, 32, 64, 64, 32, 32)[k]
+        push(ptile(col, 0, n), px_s.at[k], px_r.at[k], {"col": mate}).wait_recv()
+
+    for k in range(3):
+        px(k).start()
 
     pltpu.make_async_copy(dat, dat, a1_r).wait()
     data = dat[...].reshape(4 * LOC, GRP)
@@ -223,35 +304,13 @@
 
     pltpu.make_async_copy(snd2.at[row], dat2.at[row], a2_r).start()
 
-    def a2_send(o, c):
-        to = lax.rem(row + o, ROWS)
+    def a2_send(i, c):
+        to = at(far(i // NY), lax.rem(y + lax.rem(i + 1, NY), NY))
         pltpu.make_async_remote_copy(src_ref=snd2.at[to], dst_ref=dat2.at[row], send_sem=a2_s, recv_sem=a2_r, device_id={"row": to}, device_id_type=MESH).start()
         return c
 
-    lax.fori_loop(1, ROWS, a2_send, 0)
-
-    pltpu.make_async_copy(pgx.at[pl.ds(0, 3 * NZ)], pgx.at[pl.ds(0, 3 * NZ)], py_r).wait()
-
-    def ptile(c, lo=0, n=ROWS):
-        return pt.at[pl.ds(lo, n), pl.ds(pl.multiple_of(lax.rem(c, 2) * 16, 16), 16), pl.ds(pl.multiple_of((c // 2) * GRP, GRP), GRP)]
-
-    mine = pltpu.make_async_copy(pgx, ptile(col), ld.at[8])
-    mine.start()
-    mine.wait()
-
-    def px(k):
-        who = (col, col, col, xl * 2 + core, xr * 2 + core, xl * 2 + core, xr * 2 + core, xo * 2 + core, xo * 2 + core)[k]
-        lo = (0, 0, 0, 0, 32, 0, 0, 0, 32)[k]
-        n = (64, 64, 64, 32, 32, 64, 64, 32, 32)[k]
-        peer = (right, left, mate, right, left, mate, mate, mate, mate)[k]
-        return push(ptile(who, lo, n), px_s.at[k], px_r.at[k], peer)
-
-    def px_arrived(k):
-        n = (64, 64, 64, 32, 32, 64, 64, 32, 32)[k]
-        push(ptile(col, 0, n), px_s.at[k], px_r.at[k], mate).wait_recv()
-
-    for k in range(3):
-        px(k).start()
+    lax.fori_loop(0, ROWS - 1, a2_send, 0)
+
     px_arrived(0)
     px(3).start()
     px(5).start()
@@ -274,9 +333,15 @@
     for n in range(8):
         out_ref[0, :, 256 * n : 256 * n + 256] = bdot(lhs, pt[8 * n : 8 * n + 8].reshape(256, FW)).astype(BF)
 
+    for t in range(2):
+        for k in range(4):
+            along_x(t, k).wait_send()
+    for k in range(5):
+        for d in range(2 if k else 0):
+            along_y(d, k).wait_send()
+        for t in range(4):
+            to_mate(t, k).wait_send()
     for t in range(GROUPS):
-        for k in range(9):
-            pin(t, k, gs[t]).wait_send()
         n = NZ - 1 if t == 0 else NZ
         pltpu.make_async_copy(snd.at[t, pl.ds(0, n)], snd.at[t, pl.ds(0, n)], a1_s.at[t]).wait()
     for k in range(9):
@@ -299,7 +364,7 @@
         scratch_shapes=[
             pltpu.VMEM((LOC, D), BF),
             pltpu.VMEM((D, FW), BF),
-            pltpu.VMEM((FW, 32), BF),
+            pltpu.VMEM((32, FW), BF),
             pltpu.VMEM((64, 256), BF),
             pltpu.VMEM((2 * LOC, 4 * LOC), BF),
             pltpu.VMEM((2, LOC, GRP), F32),
@@ -314,8 +379,13 @@
             pltpu.VMEM((ROWS, 3, 4, GRP), BF),
             pltpu.VMEM((ROWS, 16, GRP), BF),
             dma((9,)),
-            dma((GROUPS, 9)),
-            dma((GROUPS, 9)),
+            pltpu.SemaphoreType.REGULAR((4,)),
+            dma((2, 4)),
+            dma((2, 4)),
+            dma((2, 5)),
+            dma((2, 5)),
+            dma((4, 5)),
+            dma((4, 5)),
             dma((GROUPS,)),
             dma,
             dma,
@@ -331,7 +401,7 @@
     )(
         tokens,
         proj_in,
-        proj_out,
+        proj_out.T,
         jnp.asarray(chan, BF),
         jnp.asarray(first, BF),
         jnp.asarray(twist, F32),

time: 77 us -> 54.9 us (0.71)
  the two profiles are of different devices: /device:TPU:1 before, /device:TPU:2 now
where the time goes in v2:
time: 54.9 us; the launch traced here: 54.8 us
  Pallas kernels  52.7 us (96%)
  local copies, waits for them, and re-layouts  2.09 us (4%)
    pallas_call x1, Pallas kernels, shards(): pl.pallas_call(kernel, out_shape=jax.ShapeDtypeStruct((1, LOC, D), BF), i...  52.7 us
    unnamed x1, local copies, waits for them, and re-layouts  2.09 us

profile of v2, /device:TPU:2, one launch (start us, length us, event | category | flops | bytes accessed | tf_op | source)
XLA Modules:
  0.0 54.8 jit_solution(14907861664631166367)
XLA Ops:
  0.0 52.7 %shard_map.73 = bf16[1,192,2048]{2,1,0:T(8,128)(2,1)} custom-call(bf16[1,192,2048]{2,1,0:T(8,128)(2,1)} %tok_hbm.1, bf16[256,512]{1,0:T(8,128)(2,1)} %win_hbm.1, bf16[32,512]{1,0:T(8,128)(2,1)} %bitcast.1, bf16[64,256]{1,0:T(8,128)(2,1)} %constant.8.clone.chan_hbm, bf16[384,768]{1,0:T(8,128)(2,1)} %constant.9.clone.first_hbm, ...), custom_call_target="tpu_custom_call" | custom-call | tf_op jit(solution)/shard_map/pallas_call | solution.py:359
  52.7 2.1 %copy.9 = bf16[1,192,2048]{2,1,0:T(8,128)(2,1)} copy(bf16[1,192,2048]{2,1,0:T(8,128)(2,1)} %shard_map.73) | data formatting | bytes 1572864

commit v3 on v2

v3 whole, which is shorter than its diff:
```python
import math

import jax
import jax.numpy as jnp
import numpy as np
from jax import lax
from jax.experimental import pallas as pl
from jax.experimental.pallas import tpu as pltpu
from jax.sharding import PartitionSpec as P

MESH = pl.DeviceIdType.MESH
GRP = 128
GROUPS = 4
NZ, NY, NX = 16, 4, 4
ROWS = NZ * NY
LOC = 192
LEN = ROWS * LOC
D = 2048
KS = 256
FW = GROUPS * GRP
F32 = jnp.float32
BF = jnp.bfloat16


def tables():
    s = np.arange(64)[:, None]
    f = np.arange(GRP)[None, :]
    ang = 2 * np.pi * ((s * f) % GRP) / GRP
    part_a = np.cos(ang)
    part_b = np.sin(ang)
    part_b[0] = np.cos(np.pi * np.arange(GRP))
    chan = np.concatenate([part_a, part_b], 1)
    q = np.arange(LOC)[:, None]
    p1 = np.arange(LOC)[None, :]
    ang = 2 * np.pi * ((q * p1) % LOC) / LOC
    first = np.repeat(np.concatenate([np.cos(ang), np.sin(ang)], 0), 4, axis=1)
    q2 = np.arange(64)[None, :]
    ang = 2 * np.pi * ((q * q2) % LEN) / LEN
    scale = 1.0 / math.sqrt(GRP * LEN)
    twist = np.stack([np.tile(np.cos(ang), (1, 2)), np.tile(np.sin(ang), (1, 2))]) * scale
    r = np.arange(64)[:, None]
    ang = 2 * np.pi * ((r * q2) % 64) / 64
    c, n = np.cos(ang), np.sin(ang)
    last = np.repeat(np.concatenate([c, n, -n, c], 1), 4, axis=0)
    return chan, first, twist, last


def bdot(a, b):
    return lax.dot_general(a, b, (((1,), (1,)), ((), ())), preferred_element_type=F32)


def kernel(tok_hbm, win_hbm, pout_hbm, chan_hbm, first_hbm, twist_hbm, last_hbm, lhs_ref, pt, tok, wfull, pblk, chan, first, twist, last, m1, l3, blk, snd, dat, snd2, dat2, ld, hops, pin_s, pin_r, yin_s, yin_r, ymt_s, ymt_r, a1_s, a1_r, a2_s, a2_r, pz_s, pz_r, py_s, py_r, px_s, px_r):
    row = lax.axis_index("row")
    col = lax.axis_index("col")
    z, y = row // NY, lax.rem(row, NY)
    x, core = col // 2, lax.rem(col, 2)
    xr = lax.rem(x + 1, NX)
    xl = lax.rem(x + NX - 1, NX)
    xo = lax.rem(x + 2, NX)
    right, left, mate = xr * 2 + core, xl * 2 + core, x * 2 + (1 - core)
    yu, yd, yo = lax.rem(y + 1, NY), lax.rem(y + NY - 1, NY), lax.rem(y + 2, NY)

    def at(dz, yy):
        return lax.rem(z + dz, NZ) * NY + yy

    bar = pltpu.get_barrier_semaphore()
    for peer in (right, left, xo * 2 + core, mate):
        pl.semaphore_signal(bar, inc=1, device_id={"col": peer}, device_id_type=MESH)
    for peer in (at(0, yu), at(0, yd), at(1, y), at(NZ - 1, y)):
        pl.semaphore_signal(bar, inc=1, device_id={"row": peer}, device_id_type=MESH)

    loads = [
        pltpu.make_async_copy(win_hbm, wfull.at[pl.ds(pl.multiple_of(col * KS, KS), KS), :], ld.at[0]),
        pltpu.make_async_copy(pout_hbm, pblk, ld.at[1]),
        pltpu.make_async_copy(tok_hbm.at[0], tok, ld.at[2]),
        pltpu.make_async_copy(chan_hbm, chan, ld.at[3]),
        pltpu.make_async_copy(first_hbm, first, ld.at[4]),
        pltpu.make_async_copy(last_hbm, last, ld.at[5]),
        pltpu.make_async_copy(twist_hbm, twist, ld.at[6]),
    ]
    for c in loads:
        c.start()
    pl.semaphore_wait(bar, 8)

    def tell(i, peers):
        for peer in peers:
            pl.semaphore_signal(hops.at[i], inc=1, device_id={"row": peer}, device_id_type=MESH)

    tell(0, (at(1, y), at(NZ - 1, y), at(0, yu), at(0, yd)))
    loads[0].wait()

    same = [col, xl * 2 + core, xr * 2 + core, xo * 2 + core]

    def tile(c, g):
        return wfull.at[pl.ds(pl.multiple_of(c * KS, KS), KS), pl.ds(pl.multiple_of(g * GRP, GRP), GRP)]

    def push(ref, ss, rs, peer):
        return pltpu.make_async_remote_copy(src_ref=ref, dst_ref=ref, send_sem=ss, recv_sem=rs, device_id=peer, device_id_type=MESH)

    order = (y, yo, yu, yd)

    def along_x(t, k):
        return push(tile(col, order[t]), pin_s.at[t, k], pin_r.at[t, k], {"col": (right, left, xo * 2 + core)[k]})

    def to_mate(t, k):
        return push(tile(same[k], order[t]), ymt_s.at[t, k], ymt_r.at[t, k], {"col": mate})

    def from_mate(t, k):
        push(tile(same[k] + 1 - 2 * core, order[t]), ymt_s.at[t, k], ymt_r.at[t, k], {"col": mate}).wait_recv()

    def along_y(d, k):
        return push(tile(same[k], y), yin_s.at[d, k - 1], yin_r.at[d, k - 1], {"row": at(0, (yu, yd)[d])})

    def y_passed(d, k):
        push(tile(same[k], (yd, yu)[d]), yin_s.at[d, k - 1], yin_r.at[d, k - 1], {"row": at(0, (yu, yd)[d])}).wait_recv()
        to_mate(3 - d, k).start()

    def x_passed(t, k):
        along_x(t, k).wait_recv()
        to_mate(t, k + 1).start()
        if t == 0:
            along_y(0, k + 1).start()
            along_y(1, k + 1).start()

    for k in range(3):
        along_x(0, k).start()
    to_mate(0, 0).start()

    rid = lax.broadcasted_iota(jnp.int32, (FW, FW), 1)
    fid = lax.broadcasted_iota(jnp.int32, (FW, FW), 0)
    inner = lax.rem(rid, 256)
    slot = (inner // 16) * 4 + lax.rem(inner, 4)
    upper = jnp.where(slot == 0, 64, GRP - slot)
    want = lax.rem(inner // 4, 4) * GRP + jnp.where(rid < 256, slot, upper)
    perm = jnp.where(fid == want, 1.0, 0.0).astype(BF)
    loads[1].wait()
    blk[...] = jnp.dot(pblk[...], perm, preferred_element_type=F32).astype(BF)

    half = pl.ds(pl.multiple_of(core * 16, 16), 16)
    quarter = pl.ds(pl.multiple_of(x * GRP, GRP), GRP)

    def mine(yy, c=None):
        c = col if c is None else c
        return pt.at[yy, :, pl.ds(pl.multiple_of(lax.rem(c, 2) * 16, 16), 16), pl.ds(pl.multiple_of((c // 2) * GRP, GRP), GRP)]

    own = pltpu.make_async_copy(blk.at[half, quarter], pt.at[y, z, half, quarter], ld.at[7])
    own.start()

    def pz_send(dz):
        pltpu.make_async_remote_copy(src_ref=blk.at[half, quarter], dst_ref=pt.at[y, z, half, quarter], send_sem=pz_s, recv_sem=pz_r, device_id={"row": at(dz, y)}, device_id_type=MESH).start()

    pl.semaphore_wait(hops.at[0], 4)
    tell(1, (at(2, y), at(NZ - 2, y)))
    for dz in (1, 15, 2, 14):
        pz_send(dz)

    for i in (3, 4, 5, 6):
        loads[i].wait()
    lane = lax.rem(lax.broadcasted_iota(jnp.int32, (2 * LOC, 4 * LOC), 1), 4)
    sub = lax.rem(lax.broadcasted_iota(jnp.int32, (256, 256), 0), 4)
    for s in range(4):
        m1[s] = first[...] * jnp.where(lane == s, 1.0, 0.0).astype(BF)
        l3[s] = last[...] * jnp.where(sub == s, 1.0, 0.0).astype(BF)

    pl.semaphore_wait(hops.at[1], 2)
    tell(2, (at(4, y), at(NZ - 4, y)))
    for dz in (3, 13, 4, 12):
        pz_send(dz)

    for k in range(3):
        x_passed(0, k)
        if k == 1:
            for j in range(3):
                along_x(1, j).start()
            for t in range(1, 4):
                to_mate(t, 0).start()

    pl.semaphore_wait(hops.at[2], 2)
    tell(3, (at(0, yu), at(0, yd), at(0, yo)))
    for dz in (8, 7, 9, 6, 10, 5, 11):
        pz_send(dz)
    own.wait()
    loads[2].wait()

    def far(i):
        step = (i + 1) // 2
        return lax.rem(8 + step * (1 - 2 * lax.rem(i, 2)) + NZ, NZ)

    peers_y = (yu, yd, yo)

    def py(o):
        return push(mine(y), py_s.at[o], py_r.at[o], {"row": at(0, peers_y[o])})

    def py_passed(o):
        push(mine((yd, yu, yo)[o]), py_s.at[o], py_r.at[o], {"row": row}).wait_recv()
        px_out(o + 1)

    whose = (y, yd, yu, yo)

    def px(u, k):
        c = (col, col, col, col, xl * 2 + core, xr * 2 + core, xo * 2 + core)[k]
        peer = (right, left, xo * 2 + core, mate, mate, mate, mate)[k]
        return push(mine(whose[u], c), px_s.at[u, k], px_r.at[u, k], {"col": peer})

    def px_out(u):
        for k in range(4):
            px(u, k).start()

    def px_passed(u):
        for k in range(3):
            px(u, k).wait_recv()
            px(u, k + 4).start()

    for t in range(GROUPS):
        g = order[t]
        if t == 1:
            pl.semaphore_wait(hops.at[3], 3)
            for k in range(3):
                x_passed(1, k)
            for k in (1, 2):
                for d in range(2):
                    y_passed(d, k)
        if t == 2:
            for d in range(2):
                y_passed(d, 3)
            part = pt.at[y, pl.ds(0, NZ - 1), half, quarter]
            pltpu.make_async_copy(part, part, pz_r).wait()
            for o in range(3):
                py(o).start()
            px_out(0)
        for k in range(4):
            from_mate(t, k)
        w = wfull[:, pl.ds(pl.multiple_of(g * GRP, GRP), GRP)]
        mapped = jnp.dot(tok[...], w, preferred_element_type=F32).astype(BF)
        zero = jnp.zeros((64, GRP), BF)
        parts = []
        for m in range(3):
            piece = mapped[64 * m : 64 * m + 64]
            parts.append(jnp.concatenate([piece, zero], 1))
            parts.append(jnp.concatenate([zero, piece], 1))
        spread = bdot(chan[...], jnp.concatenate(parts, 0))
        for m in range(3):
            snd[t, :, m] = spread[:, GRP * m : GRP * m + GRP].reshape(NZ, 4, GRP).astype(BF)

        def a1_send(i, c, t=t, g=g):
            to = lax.rem(z + far(i), NZ)
            pltpu.make_async_remote_copy(src_ref=snd.at[t, to], dst_ref=dat.at[row], send_sem=a1_s.at[t], recv_sem=a1_r, device_id={"row": to * NY + g}, device_id_type=MESH).start()
            return c

        lax.fori_loop(0, NZ - 1 if t == 0 else NZ, a1_send, 0)
        if t == 0:
            pltpu.make_async_copy(snd.at[0, z], dat.at[row], a1_r).start()

    for t in range(2):
        for k in range(3):
            along_x(t, k).wait_send()
    for k in range(4):
        for t in range(4):
            to_mate(t, k).wait_send()
        if k:
            for d in range(2):
                along_y(d, k).wait_send()

    for o in range(3):
        py_passed(o)

    pltpu.make_async_copy(dat, dat, a1_r).wait()
    data = dat[...].reshape(4 * LOC, GRP)
    cc, sn = twist[0], twist[1]
    first_slot = z == 0
    lanes = lax.broadcasted_iota(jnp.int32, (1, GRP), 1) < 64
    sgn = jnp.where(lanes, 1.0, -1.0)
    zero_b = jnp.where(lanes, 1.0, 0.0)
    spec = jnp.where(first_slot, 1.0, 0.0)
    outs = [None] * 3
    for s in range(4):
        got = jnp.dot(m1[s], data, preferred_element_type=F32)
        re, im = got[:LOC], got[LOC:]
        tre = re * cc - im * sn
        tim = re * sn + im * cc
        if s == 0:
            lo_mask = zero_b * spec + sgn * (1.0 - spec)
            up_keep, up_turn = 1.0 - spec, zero_b * spec
            lo_re, lo_im = tre * lo_mask, tim * lo_mask
            up_re = tre * up_keep + pltpu.roll(tre, 64, 1) * up_turn
            up_im = tim * up_keep + pltpu.roll(tim, 64, 1) * up_turn
        else:
            lo_re, lo_im, up_re, up_im = tre * sgn, tim * sgn, tre, tim
        lo = jnp.concatenate([lo_re, lo_im], 1).astype(BF)
        up = jnp.concatenate([up_re, up_im], 1).astype(BF)
        for m in range(3):
            rhs = jnp.concatenate([lo[64 * m : 64 * m + 64], up[64 * m : 64 * m + 64]], 0)
            term = bdot(l3[s], rhs)
            outs[m] = term if outs[m] is None else outs[m] + term
    for m in range(3):
        snd2[:, m] = outs[m].reshape(ROWS, 4, GRP).astype(BF)

    pltpu.make_async_copy(snd2.at[row], dat2.at[row], a2_r).start()

    def a2_send(i, c):
        to = at(far(i // NY), lax.rem(y + lax.rem(i + 1, NY), NY))
        pltpu.make_async_remote_copy(src_ref=snd2.at[to], dst_ref=dat2.at[row], send_sem=a2_s, recv_sem=a2_r, device_id={"row": to}, device_id_type=MESH).start()
        return c

    lax.fori_loop(0, ROWS - 1, a2_send, 0)

    for u in range(4):
        px_passed(u)
    for u in range(4):
        for k in range(3, 7):
            px(u, k).wait_recv()

    for t in range(GROUPS):
        n = NZ - 1 if t == 0 else NZ
        pltpu.make_async_copy(snd.at[t, pl.ds(0, n)], snd.at[t, pl.ds(0, n)], a1_s.at[t]).wait()
    for u in range(4):
        for k in range(7):
            px(u, k).wait_send()
    pltpu.make_async_copy(part, part, pz_s).wait()
    for o in range(3):
        py(o).wait_send()
    pltpu.make_async_copy(snd2.at[pl.ds(0, ROWS - 1)], snd2.at[pl.ds(0, ROWS - 1)], a2_s).wait()

    pltpu.make_async_copy(dat2, dat2, a2_r).wait()
    sides = []
    for m in range(3):
        t = dat2[:, m].reshape(256, GRP).T
        sides.append(jnp.concatenate([t[:64], t[64:]], 1))
    lhs = jnp.concatenate(sides, 0)
    lhs_ref[...] = lhs


def product(lhs_ref, pt_ref, out_hbm, out, sem):
    wide = D // 8
    copies = []
    for n in range(8):
        cols = pl.ds(wide * n, wide)
        rhs = jnp.concatenate([pt_ref[yy, zz] for zz in (2 * n, 2 * n + 1) for yy in range(NY)], 0)
        out[:, cols] = bdot(lhs_ref[...], rhs).astype(BF)
        copies.append(pltpu.make_async_copy(out.at[:, cols], out_hbm.at[0, :, cols], sem.at[n]))
        copies[-1].start()
    for c in copies:
        c.wait()


def shards(tokens, proj_in, proj_out):
    chan, first, twist, last = tables()
    anyspec = pl.BlockSpec(memory_space=pltpu.HBM)
    dma = pltpu.SemaphoreType.DMA
    lhs, pt = pl.pallas_call(
        kernel,
        out_shape=(jax.ShapeDtypeStruct((LOC, FW), BF), jax.ShapeDtypeStruct((NY, NZ, 32, FW), BF)),
        in_specs=[anyspec] * 7,
        out_specs=(pl.BlockSpec(memory_space=pltpu.VMEM), pl.BlockSpec(memory_space=pltpu.VMEM)),
        scratch_shapes=[
            pltpu.VMEM((LOC, D), BF),
            pltpu.VMEM((D, FW), BF),
            pltpu.VMEM((32, FW), BF),
            pltpu.VMEM((64, 256), BF),
            pltpu.VMEM((2 * LOC, 4 * LOC), BF),
            pltpu.VMEM((2, LOC, GRP), F32),
            pltpu.VMEM((256, 256), BF),
            pltpu.VMEM((4, 2 * LOC, 4 * LOC), BF),
            pltpu.VMEM((4, 256, 256), BF),
            pltpu.VMEM((32, FW), BF),
            pltpu.VMEM((GROUPS, NZ, 3, 4, GRP), BF),
            pltpu.VMEM((ROWS, 3, 4, GRP), BF),
            pltpu.VMEM((ROWS, 3, 4, GRP), BF),
            pltpu.VMEM((ROWS, 3, 4, GRP), BF),
            dma((9,)),
            pltpu.SemaphoreType.REGULAR((4,)),
            dma((2, 3)),
            dma((2, 3)),
            dma((2, 3)),
            dma((2, 3)),
            dma((4, 4)),
            dma((4, 4)),
            dma((GROUPS,)),
            dma,
            dma,
            dma,
            dma,
            dma,
            dma((3,)),
            dma((3,)),
            dma((4, 7)),
            dma((4, 7)),
        ],
        compiler_params=pltpu.CompilerParams(collective_id=0, has_side_effects=True, vmem_limit_bytes=24 << 20),
    )(
        *(
            pltpu.with_memory_space_constraint(a, pltpu.HBM)
            for a in (tokens, proj_in, proj_out.T, jnp.asarray(chan, BF), jnp.asarray(first, BF), jnp.asarray(twist, F32), jnp.asarray(last, BF))
        )
    )
    return pl.pallas_call(
        product,
        out_shape=jax.ShapeDtypeStruct((1, LOC, D), BF),
        in_specs=[pl.BlockSpec(memory_space=pltpu.VMEM)] * 2,
        out_specs=pl.BlockSpec(memory_space=pl.ANY),
        scratch_shapes=[pltpu.VMEM((LOC, D), BF), dma((8,))],
        compiler_params=pltpu.CompilerParams(vmem_limit_bytes=24 << 20),
    )(lhs, pt)


def solution(mesh):
    return jax.shard_map(
        shards,
        mesh=mesh,
        in_specs=(P("col", "row", None), P("col", None), P(None, "row")),
        out_specs=P("col", "row", None),
        check_vma=False,
    )
```

time: 54.9 us -> 51.4 us (0.936)
  the two profiles are of different devices: /device:TPU:2 before, /device:TPU:8 now
where the time goes in v3:
time: 51.4 us; the launch traced here: 51.3 us
  Pallas kernels  51.3 us (100%)
    pallas_call x1, Pallas kernels, shards(): pl.pallas_call(kernel, out_shape=(jax.ShapeDtypeStruct((LOC, FW), BF), ja...  49.7 us
    pallas_call x1, Pallas kernels, shards(): pl.pallas_call(product, out_shape=jax.ShapeDtypeStruct((1, LOC, D), BF),...  1.6 us

profile of v3, /device:TPU:8, one launch (start us, length us, event | category | flops | bytes accessed | tf_op | source)
XLA Modules:
  0.0 51.3 jit_solution(8563827887180593021)
XLA Ops:
  0.0 49.7 %shard_map.73 = (bf16[192,512]{1,0:T(8,128)(2,1)S(1)}, bf16[4,16,32,512]{3,2,1,0:T(8,128)(2,1)S(1)}) custom-call(bf16[1,192,2048]{2,1,0:T(8,128)(2,1)} %tok_hbm.1, bf16[256,512]{1,0:T(8,128)(2,1)} %win_hbm.1, bf16[32,512]{1,0:T(8,128)(2,1)} %bitcast.1, bf16[64,256]{1,0:T(8,128)(2,1)} %constant.8.clone.chan_hbm, bf16[384,768]{1,0:T(8,128)(2,1)} %constant.9.clone.first_hbm, ...), custom_call_target="tpu_custom_call" | custom-call | tf_op jit(solution)/shard_map/pallas_call | solution.py:350
  49.7 1.6 %shard_map.74 = bf16[1,192,2048]{2,1,0:T(8,128)(2,1)} custom-call(bf16[192,512]{1,0:T(8,128)(2,1)S(1)} %get-tuple-element.7.lhs_ref, bf16[4,16,32,512]{3,2,1,0:T(8,128)(2,1)S(1)} %get-tuple-element.8.pt_ref), custom_call_target="tpu_custom_call" | custom-call | tf_op jit(solution)/shard_map/pallas_call | solution.py:396

commit v4 on v3

--- a/solution.py
+++ b/solution.py
@@ -49,7 +49,7 @@
     return lax.dot_general(a, b, (((1,), (1,)), ((), ())), preferred_element_type=F32)
 
 
-def kernel(tok_hbm, win_hbm, pout_hbm, chan_hbm, first_hbm, twist_hbm, last_hbm, lhs_ref, pt, tok, wfull, pblk, chan, first, twist, last, m1, l3, blk, snd, dat, snd2, dat2, ld, hops, pin_s, pin_r, yin_s, yin_r, ymt_s, ymt_r, a1_s, a1_r, a2_s, a2_r, pz_s, pz_r, py_s, py_r, px_s, px_r):
+def kernel(tok_hbm, win_hbm, pout_hbm, chan_hbm, first_hbm, twist_hbm, last_hbm, lhs_ref, pt, tok, wfull, pblk, chan, first, twist, last, m1, l3, blk, snd, dat, snd2, dat2, ld, hops, w_s, pin_r, yin_r, ymt_r, a1_s, a1_r, a2_s, a2_r, pz_s, pz_r, p_s, py_r, px_r):
     row = lax.axis_index("row")
     col = lax.axis_index("col")
     z, y = row // NY, lax.rem(row, NY)
@@ -74,9 +74,9 @@
         pltpu.make_async_copy(pout_hbm, pblk, ld.at[1]),
         pltpu.make_async_copy(tok_hbm.at[0], tok, ld.at[2]),
         pltpu.make_async_copy(chan_hbm, chan, ld.at[3]),
-        pltpu.make_async_copy(first_hbm, first, ld.at[4]),
-        pltpu.make_async_copy(last_hbm, last, ld.at[5]),
-        pltpu.make_async_copy(twist_hbm, twist, ld.at[6]),
+        pltpu.make_async_copy(first_hbm, first, ld.at[3]),
+        pltpu.make_async_copy(last_hbm, last, ld.at[3]),
+        pltpu.make_async_copy(twist_hbm, twist, ld.at[3]),
     ]
     for c in loads:
         c.start()
@@ -94,37 +94,26 @@
     def tile(c, g):
         return wfull.at[pl.ds(pl.multiple_of(c * KS, KS), KS), pl.ds(pl.multiple_of(g * GRP, GRP), GRP)]
 
+    def arrived(rows, sem):
+        pltpu.make_async_copy(wfull.at[pl.ds(0, rows)], wfull.at[pl.ds(0, rows)], sem).wait()
+
     def push(ref, ss, rs, peer):
         return pltpu.make_async_remote_copy(src_ref=ref, dst_ref=ref, send_sem=ss, recv_sem=rs, device_id=peer, device_id_type=MESH)
 
     order = (y, yo, yu, yd)
 
     def along_x(t, k):
-        return push(tile(col, order[t]), pin_s.at[t, k], pin_r.at[t, k], {"col": (right, left, xo * 2 + core)[k]})
+        return push(tile(col, order[t]), w_s, pin_r.at[k if t == 0 else 3], {"col": (right, left, xo * 2 + core)[k]})
 
     def to_mate(t, k):
-        return push(tile(same[k], order[t]), ymt_s.at[t, k], ymt_r.at[t, k], {"col": mate})
-
-    def from_mate(t, k):
-        push(tile(same[k] + 1 - 2 * core, order[t]), ymt_s.at[t, k], ymt_r.at[t, k], {"col": mate}).wait_recv()
+        push(tile(same[k], order[t]), w_s, ymt_r.at[t], {"col": mate}).start()
 
     def along_y(d, k):
-        return push(tile(same[k], y), yin_s.at[d, k - 1], yin_r.at[d, k - 1], {"row": at(0, (yu, yd)[d])})
-
-    def y_passed(d, k):
-        push(tile(same[k], (yd, yu)[d]), yin_s.at[d, k - 1], yin_r.at[d, k - 1], {"row": at(0, (yu, yd)[d])}).wait_recv()
-        to_mate(3 - d, k).start()
-
-    def x_passed(t, k):
-        along_x(t, k).wait_recv()
-        to_mate(t, k + 1).start()
-        if t == 0:
-            along_y(0, k + 1).start()
-            along_y(1, k + 1).start()
+        push(tile(same[k], y), w_s, yin_r.at[k // 3], {"row": at(0, (yu, yd)[d])}).start()
 
     for k in range(3):
         along_x(0, k).start()
-    to_mate(0, 0).start()
+    to_mate(0, 0)
 
     rid = lax.broadcasted_iota(jnp.int32, (FW, FW), 1)
     fid = lax.broadcasted_iota(jnp.int32, (FW, FW), 0)
@@ -143,7 +132,7 @@
         c = col if c is None else c
         return pt.at[yy, :, pl.ds(pl.multiple_of(lax.rem(c, 2) * 16, 16), 16), pl.ds(pl.multiple_of((c // 2) * GRP, GRP), GRP)]
 
-    own = pltpu.make_async_copy(blk.at[half, quarter], pt.at[y, z, half, quarter], ld.at[7])
+    own = pltpu.make_async_copy(blk.at[half, quarter], pt.at[y, z, half, quarter], ld.at[4])
     own.start()
 
     def pz_send(dz):
@@ -154,8 +143,7 @@
     for dz in (1, 15, 2, 14):
         pz_send(dz)
 
-    for i in (3, 4, 5, 6):
-        loads[i].wait()
+    arrived(928, ld.at[3])
     lane = lax.rem(lax.broadcasted_iota(jnp.int32, (2 * LOC, 4 * LOC), 1), 4)
     sub = lax.rem(lax.broadcasted_iota(jnp.int32, (256, 256), 0), 4)
     for s in range(4):
@@ -168,12 +156,15 @@
         pz_send(dz)
 
     for k in range(3):
-        x_passed(0, k)
+        arrived(64, pin_r.at[k])
+        to_mate(0, k + 1)
+        along_y(0, k + 1)
+        along_y(1, k + 1)
         if k == 1:
             for j in range(3):
                 along_x(1, j).start()
             for t in range(1, 4):
-                to_mate(t, 0).start()
+                to_mate(t, 0)
 
     pl.semaphore_wait(hops.at[2], 2)
     tell(3, (at(0, yu), at(0, yd), at(0, yo)))
@@ -186,50 +177,36 @@
         step = (i + 1) // 2
         return lax.rem(8 + step * (1 - 2 * lax.rem(i, 2)) + NZ, NZ)
 
-    peers_y = (yu, yd, yo)
-
-    def py(o):
-        return push(mine(y), py_s.at[o], py_r.at[o], {"row": at(0, peers_y[o])})
-
-    def py_passed(o):
-        push(mine((yd, yu, yo)[o]), py_s.at[o], py_r.at[o], {"row": row}).wait_recv()
-        px_out(o + 1)
-
-    whose = (y, yd, yu, yo)
-
     def px(u, k):
         c = (col, col, col, col, xl * 2 + core, xr * 2 + core, xo * 2 + core)[k]
         peer = (right, left, xo * 2 + core, mate, mate, mate, mate)[k]
-        return push(mine(whose[u], c), px_s.at[u, k], px_r.at[u, k], {"col": peer})
+        push(mine(order[u], c), p_s, px_r.at[u if k < 3 else 4], {"col": peer}).start()
 
     def px_out(u):
         for k in range(4):
-            px(u, k).start()
-
-    def px_passed(u):
-        for k in range(3):
-            px(u, k).wait_recv()
-            px(u, k + 4).start()
+            px(u, k)
 
     for t in range(GROUPS):
         g = order[t]
         if t == 1:
             pl.semaphore_wait(hops.at[3], 3)
-            for k in range(3):
-                x_passed(1, k)
+            arrived(192, pin_r.at[3])
+            for k in (1, 2, 3):
+                to_mate(1, k)
+            arrived(256, yin_r.at[0])
             for k in (1, 2):
-                for d in range(2):
-                    y_passed(d, k)
+                to_mate(2, k)
+                to_mate(3, k)
         if t == 2:
-            for d in range(2):
-                y_passed(d, 3)
+            arrived(128, yin_r.at[1])
+            to_mate(2, 3)
+            to_mate(3, 3)
             part = pt.at[y, pl.ds(0, NZ - 1), half, quarter]
             pltpu.make_async_copy(part, part, pz_r).wait()
             for o in range(3):
-                py(o).start()
+                push(mine(y), p_s, py_r, {"row": at(0, order[o + 1])}).start()
             px_out(0)
-        for k in range(4):
-            from_mate(t, k)
+        arrived(256, ymt_r.at[t])
         w = wfull[:, pl.ds(pl.multiple_of(g * GRP, GRP), GRP)]
         mapped = jnp.dot(tok[...], w, preferred_element_type=F32).astype(BF)
         zero = jnp.zeros((64, GRP), BF)
@@ -244,25 +221,16 @@
 
         def a1_send(i, c, t=t, g=g):
             to = lax.rem(z + far(i), NZ)
-            pltpu.make_async_remote_copy(src_ref=snd.at[t, to], dst_ref=dat.at[row], send_sem=a1_s.at[t], recv_sem=a1_r, device_id={"row": to * NY + g}, device_id_type=MESH).start()
+            pltpu.make_async_remote_copy(src_ref=snd.at[t, to], dst_ref=dat.at[row], send_sem=a1_s, recv_sem=a1_r, device_id={"row": to * NY + g}, device_id_type=MESH).start()
             return c
 
         lax.fori_loop(0, NZ - 1 if t == 0 else NZ, a1_send, 0)
         if t == 0:
             pltpu.make_async_copy(snd.at[0, z], dat.at[row], a1_r).start()
 
-    for t in range(2):
-        for k in range(3):
-            along_x(t, k).wait_send()
-    for k in range(4):
-        for t in range(4):
-            to_mate(t, k).wait_send()
-        if k:
-            for d in range(2):
-                along_y(d, k).wait_send()
-
-    for o in range(3):
-        py_passed(o)
+    arrived(192, py_r)
+    for u in (1, 2, 3):
+        px_out(u)
 
     pltpu.make_async_copy(dat, dat, a1_r).wait()
     data = dat[...].reshape(4 * LOC, GRP)
@@ -305,21 +273,16 @@
     lax.fori_loop(0, ROWS - 1, a2_send, 0)
 
     for u in range(4):
-        px_passed(u)
-    for u in range(4):
-        for k in range(3, 7):
-            px(u, k).wait_recv()
-
-    for t in range(GROUPS):
-        n = NZ - 1 if t == 0 else NZ
-        pltpu.make_async_copy(snd.at[t, pl.ds(0, n)], snd.at[t, pl.ds(0, n)], a1_s.at[t]).wait()
-    for u in range(4):
-        for k in range(7):
-            px(u, k).wait_send()
+        arrived(192, px_r.at[u])
+        for k in (4, 5, 6):
+            px(u, k)
+
+    arrived(28 * 64, w_s)
     pltpu.make_async_copy(part, part, pz_s).wait()
-    for o in range(3):
-        py(o).wait_send()
-    pltpu.make_async_copy(snd2.at[pl.ds(0, ROWS - 1)], snd2.at[pl.ds(0, ROWS - 1)], a2_s).wait()
+    arrived(31 * 64, p_s)
+    for sem in (a1_s, a2_s):
+        pltpu.make_async_copy(dat.at[pl.ds(0, ROWS - 1)], dat.at[pl.ds(0, ROWS - 1)], sem).wait()
+    arrived(1024, px_r.at[4])
 
     pltpu.make_async_copy(dat2, dat2, a2_r).wait()
     sides = []
@@ -367,24 +330,21 @@
             pltpu.VMEM((ROWS, 3, 4, GRP), BF),
             pltpu.VMEM((ROWS, 3, 4, GRP), BF),
             pltpu.VMEM((ROWS, 3, 4, GRP), BF),
-            dma((9,)),
+            dma((5,)),
             pltpu.SemaphoreType.REGULAR((4,)),
-            dma((2, 3)),
-            dma((2, 3)),
-            dma((2, 3)),
-            dma((2, 3)),
-            dma((4, 4)),
-            dma((4, 4)),
-            dma((GROUPS,)),
-            dma,
-            dma,
-            dma,
-            dma,
-            dma,
-            dma((3,)),
-            dma((3,)),
-            dma((4, 7)),
-            dma((4, 7)),
+            dma,
+            dma((4,)),
+            dma((2,)),
+            dma((4,)),
+            dma,
+            dma,
+            dma,
+            dma,
+            dma,
+            dma,
+            dma,
+            dma,
+            dma((5,)),
         ],
         compiler_params=pltpu.CompilerParams(collective_id=0, has_side_effects=True, vmem_limit_bytes=24 << 20),
     )(

time: 51.4 us -> 50.6 us (0.984)
  Pallas kernels: 51.3 us -> 50.5 us
    pallas_call x1, Pallas kernels: 49.7 us -> 48.9 us  [shards(): pl.pallas_call(kernel, out_shape=(jax.ShapeDtypeStruct((LOC, FW), BF), ja...]
where the time goes in v4:
time: 50.6 us; the launch traced here: 50.5 us
  Pallas kernels  50.5 us (100%)
    pallas_call x1, Pallas kernels, shards(): pl.pallas_call(kernel, out_shape=(jax.ShapeDtypeStruct((LOC, FW), BF), ja...  48.9 us
    pallas_call x1, Pallas kernels, shards(): pl.pallas_call(product, out_shape=jax.ShapeDtypeStruct((1, LOC, D), BF),...  1.6 us

profile of v4, /device:TPU:8, one launch (start us, length us, event | category | flops | bytes accessed | tf_op | source)
XLA Modules:
  0.0 50.5 jit_solution(1688043487006668299)
XLA Ops:
  0.0 48.9 %shard_map.73 = (bf16[192,512]{1,0:T(8,128)(2,1)S(1)}, bf16[4,16,32,512]{3,2,1,0:T(8,128)(2,1)S(1)}) custom-call(bf16[1,192,2048]{2,1,0:T(8,128)(2,1)} %tok_hbm.1, bf16[256,512]{1,0:T(8,128)(2,1)} %win_hbm.1, bf16[32,512]{1,0:T(8,128)(2,1)} %bitcast.1, bf16[64,256]{1,0:T(8,128)(2,1)} %constant.8.clone.chan_hbm, bf16[384,768]{1,0:T(8,128)(2,1)} %constant.9.clone.first_hbm, ...), custom_call_target="tpu_custom_call" | custom-call | tf_op jit(solution)/shard_map/pallas_call | solution.py:313
  48.9 1.6 %shard_map.74 = bf16[1,192,2048]{2,1,0:T(8,128)(2,1)} custom-call(bf16[192,512]{1,0:T(8,128)(2,1)S(1)} %get-tuple-element.7.lhs_ref, bf16[4,16,32,512]{3,2,1,0:T(8,128)(2,1)S(1)} %get-tuple-element.8.pt_ref), custom_call_target="tpu_custom_call" | custom-call | tf_op jit(solution)/shard_map/pallas_call | solution.py:356

commit v5 on v4

--- a/solution.py
+++ b/solution.py
@@ -31,9 +31,12 @@
     part_b[0] = np.cos(np.pi * np.arange(GRP))
     chan = np.concatenate([part_a, part_b], 1)
     q = np.arange(LOC)[:, None]
-    p1 = np.arange(LOC)[None, :]
-    ang = 2 * np.pi * ((q * p1) % LOC) / LOC
-    first = np.repeat(np.concatenate([np.cos(ang), np.sin(ang)], 0), 4, axis=1)
+    halves = []
+    for e in range(2):
+        p1 = np.array([3 * (NY * zz + e + 2 * h) + m for h in range(2) for zz in range(NZ) for m in range(3)])[None, :]
+        ang = 2 * np.pi * ((q * p1) % LOC) / LOC
+        halves.append(np.repeat(np.concatenate([np.cos(ang), np.sin(ang)], 0), 4, axis=1))
+    first = np.stack(halves)
     q2 = np.arange(64)[None, :]
     ang = 2 * np.pi * ((q * q2) % LEN) / LEN
     scale = 1.0 / math.sqrt(GRP * LEN)
@@ -49,7 +52,7 @@
     return lax.dot_general(a, b, (((1,), (1,)), ((), ())), preferred_element_type=F32)
 
 
-def kernel(tok_hbm, win_hbm, pout_hbm, chan_hbm, first_hbm, twist_hbm, last_hbm, lhs_ref, pt, tok, wfull, pblk, chan, first, twist, last, m1, l3, blk, snd, dat, snd2, dat2, ld, hops, w_s, pin_r, yin_r, ymt_r, a1_s, a1_r, a2_s, a2_r, pz_s, pz_r, p_s, py_r, px_r):
+def kernel(tok_hbm, win_hbm, pout_hbm, chan_hbm, first_hbm, twist_hbm, last_hbm, lhs_ref, pt, tok, wfull, pblk, chan, first, twist, last, m1, l3, blk, snd, acc, dat, snd2, dat2, ld, hops, w_s, pin_r, yin_r, ymt_r, a1_s, a1_r, a2_s, a2_r, pz_s, pz_r, p_s, py_r, px_r):
     row = lax.axis_index("row")
     col = lax.axis_index("col")
     z, y = row // NY, lax.rem(row, NY)
@@ -144,10 +147,11 @@
         pz_send(dz)
 
     arrived(928, ld.at[3])
-    lane = lax.rem(lax.broadcasted_iota(jnp.int32, (2 * LOC, 4 * LOC), 1), 4)
+    lane = lax.rem(lax.broadcasted_iota(jnp.int32, (2 * LOC, 2 * LOC), 1), 4)
     sub = lax.rem(lax.broadcasted_iota(jnp.int32, (256, 256), 0), 4)
     for s in range(4):
-        m1[s] = first[...] * jnp.where(lane == s, 1.0, 0.0).astype(BF)
+        for e in range(2):
+            m1[e, s] = first[e] * jnp.where(lane == s, 1.0, 0.0).astype(BF)
         l3[s] = last[...] * jnp.where(sub == s, 1.0, 0.0).astype(BF)
 
     pl.semaphore_wait(hops.at[1], 2)
@@ -185,6 +189,24 @@
     def px_out(u):
         for k in range(4):
             px(u, k)
+
+    side = lax.rem(y, 2)
+
+    def groups_out(t, which):
+        def send():
+            def a1_send(i, c):
+                to = lax.rem(z + far(i), NZ)
+                pltpu.make_async_remote_copy(src_ref=snd.at[t, to], dst_ref=dat.at[side, y // 2, z], send_sem=a1_s, recv_sem=a1_r.at[t // 2], device_id={"row": to * NY + order[t]}, device_id_type=MESH).start()
+                return c
+
+            lax.fori_loop(0, NZ - 1 if t == 0 else NZ, a1_send, 0)
+            if t == 0:
+                pltpu.make_async_copy(snd.at[0, z], dat.at[side, y // 2, z], a1_r.at[0]).start()
+
+        if which is None:
+            send()
+        else:
+            pl.when(core == which)(send)
 
     for t in range(GROUPS):
         g = order[t]
@@ -219,21 +241,24 @@
         for m in range(3):
             snd[t, :, m] = spread[:, GRP * m : GRP * m + GRP].reshape(NZ, 4, GRP).astype(BF)
 
-        def a1_send(i, c, t=t, g=g):
-            to = lax.rem(z + far(i), NZ)
-            pltpu.make_async_remote_copy(src_ref=snd.at[t, to], dst_ref=dat.at[row], send_sem=a1_s, recv_sem=a1_r, device_id={"row": to * NY + g}, device_id_type=MESH).start()
-            return c
-
-        lax.fori_loop(0, NZ - 1 if t == 0 else NZ, a1_send, 0)
-        if t == 0:
-            pltpu.make_async_copy(snd.at[0, z], dat.at[row], a1_r).start()
+        for u in range(GROUPS):
+            early, late = u == t, t == min(u + 1, GROUPS - 1)
+            if early or late:
+                which = None if early and late else 1 if early else 0
+                groups_out(u, which)
 
     arrived(192, py_r)
     for u in (1, 2, 3):
         px_out(u)
 
-    pltpu.make_async_copy(dat, dat, a1_r).wait()
-    data = dat[...].reshape(4 * LOC, GRP)
+    early = dat.at[side]
+    pltpu.make_async_copy(early, early, a1_r.at[0]).wait()
+    data = early[...].reshape(2 * LOC, GRP)
+    for s in range(4):
+        acc[s] = jnp.dot(m1[side, s], data, preferred_element_type=F32)
+    late = dat.at[1 - side]
+    pltpu.make_async_copy(late, late, a1_r.at[1]).wait()
+    data = late[...].reshape(2 * LOC, GRP)
     cc, sn = twist[0], twist[1]
     first_slot = z == 0
     lanes = lax.broadcasted_iota(jnp.int32, (1, GRP), 1) < 64
@@ -242,7 +267,7 @@
     spec = jnp.where(first_slot, 1.0, 0.0)
     outs = [None] * 3
     for s in range(4):
-        got = jnp.dot(m1[s], data, preferred_element_type=F32)
+        got = acc[s] + jnp.dot(m1[1 - side, s], data, preferred_element_type=F32)
         re, im = got[:LOC], got[LOC:]
         tre = re * cc - im * sn
         tim = re * sn + im * cc
@@ -281,7 +306,7 @@
     pltpu.make_async_copy(part, part, pz_s).wait()
     arrived(31 * 64, p_s)
     for sem in (a1_s, a2_s):
-        pltpu.make_async_copy(dat.at[pl.ds(0, ROWS - 1)], dat.at[pl.ds(0, ROWS - 1)], sem).wait()
+        pltpu.make_async_copy(dat2.at[pl.ds(0, ROWS - 1)], dat2.at[pl.ds(0, ROWS - 1)], sem).wait()
     arrived(1024, px_r.at[4])
 
     pltpu.make_async_copy(dat2, dat2, a2_r).wait()
@@ -320,14 +345,15 @@
             pltpu.VMEM((D, FW), BF),
             pltpu.VMEM((32, FW), BF),
             pltpu.VMEM((64, 256), BF),
-            pltpu.VMEM((2 * LOC, 4 * LOC), BF),
+            pltpu.VMEM((2, 2 * LOC, 2 * LOC), BF),
             pltpu.VMEM((2, LOC, GRP), F32),
             pltpu.VMEM((256, 256), BF),
-            pltpu.VMEM((4, 2 * LOC, 4 * LOC), BF),
+            pltpu.VMEM((2, 4, 2 * LOC, 2 * LOC), BF),
             pltpu.VMEM((4, 256, 256), BF),
             pltpu.VMEM((32, FW), BF),
             pltpu.VMEM((GROUPS, NZ, 3, 4, GRP), BF),
-            pltpu.VMEM((ROWS, 3, 4, GRP), BF),
+            pltpu.VMEM((4, 2 * LOC, GRP), F32),
+            pltpu.VMEM((2, 2, NZ, 3, 4, GRP), BF),
             pltpu.VMEM((ROWS, 3, 4, GRP), BF),
             pltpu.VMEM((ROWS, 3, 4, GRP), BF),
             dma((5,)),
@@ -337,7 +363,7 @@
             dma((2,)),
             dma((4,)),
             dma,
-            dma,
+            dma((2,)),
             dma,
             dma,
             dma,

time: 50.6 us -> 49.3 us (0.974)
  Pallas kernels: 50.5 us -> 49.2 us
    pallas_call x1, Pallas kernels: 48.9 us -> 47.6 us  [shards(): pl.pallas_call(kernel, out_shape=(jax.ShapeDtypeStruct((LOC, FW), BF), ja...]
where the time goes in v5:
time: 49.3 us; the launch traced here: 49.2 us
  Pallas kernels  49.2 us (100%)
    pallas_call x1, Pallas kernels, shards(): pl.pallas_call(kernel, out_shape=(jax.ShapeDtypeStruct((LOC, FW), BF), ja...  47.6 us
    pallas_call x1, Pallas kernels, shards(): pl.pallas_call(product, out_shape=jax.ShapeDtypeStruct((1, LOC, D), BF),...  1.6 us

profile of v5, /device:TPU:8, one launch (start us, length us, event | category | flops | bytes accessed | tf_op | source)
XLA Modules:
  0.0 49.2 jit_solution(3862983952527194448)
XLA Ops:
  0.0 47.6 %shard_map.73 = (bf16[192,512]{1,0:T(8,128)(2,1)S(1)}, bf16[4,16,32,512]{3,2,1,0:T(8,128)(2,1)S(1)}) custom-call(bf16[1,192,2048]{2,1,0:T(8,128)(2,1)} %tok_hbm.1, bf16[256,512]{1,0:T(8,128)(2,1)} %win_hbm.1, bf16[32,512]{1,0:T(8,128)(2,1)} %bitcast.1, bf16[64,256]{1,0:T(8,128)(2,1)} %constant.8.clone.chan_hbm, ...), custom_call_target="tpu_custom_call" | custom-call | tf_op jit(solution)/shard_map/pallas_call | solution.py:338
  47.6 1.6 %shard_map.74 = bf16[1,192,2048]{2,1,0:T(8,128)(2,1)} custom-call(bf16[192,512]{1,0:T(8,128)(2,1)S(1)} %get-tuple-element.7.lhs_ref, bf16[4,16,32,512]{3,2,1,0:T(8,128)(2,1)S(1)} %get-tuple-element.8.pt_ref), custom_call_target="tpu_custom_call" | custom-call | tf_op jit(solution)/shard_map/pallas_call | solution.py:382

commit v6 on v5

--- a/solution.py
+++ b/solution.py
@@ -139,7 +139,14 @@
     own.start()
 
     def pz_send(dz):
-        pltpu.make_async_remote_copy(src_ref=blk.at[half, quarter], dst_ref=pt.at[y, z, half, quarter], send_sem=pz_s, recv_sem=pz_r, device_id={"row": at(dz, y)}, device_id_type=MESH).start()
+        rs = pz_r.at[{4: 1, 12: 2}.get(dz, 0)]
+        pltpu.make_async_remote_copy(src_ref=blk.at[half, quarter], dst_ref=pt.at[y, z, half, quarter], send_sem=pz_s, recv_sem=rs, device_id={"row": at(dz, y)}, device_id_type=MESH).start()
+
+    def pz_relay(i):
+        ref = pt.at[y, lax.rem(z + (12, 4)[i], NZ), half, quarter]
+        pltpu.make_async_copy(ref, ref, pz_r.at[i + 1]).wait()
+        for dz in ((3, 2, 1), (12, 13, 14, 15))[i]:
+            push(ref, pz_s, pz_r.at[0], {"row": at(dz, y)}).start()
 
     pl.semaphore_wait(hops.at[0], 4)
     tell(1, (at(2, y), at(NZ - 2, y)))
@@ -172,10 +179,10 @@
 
     pl.semaphore_wait(hops.at[2], 2)
     tell(3, (at(0, yu), at(0, yd), at(0, yo)))
-    for dz in (8, 7, 9, 6, 10, 5, 11):
-        pz_send(dz)
     own.wait()
     loads[2].wait()
+    for i in range(2):
+        pz_relay(i)
 
     def far(i):
         step = (i + 1) // 2
@@ -223,8 +230,8 @@
             arrived(128, yin_r.at[1])
             to_mate(2, 3)
             to_mate(3, 3)
-            part = pt.at[y, pl.ds(0, NZ - 1), half, quarter]
-            pltpu.make_async_copy(part, part, pz_r).wait()
+            part = pt.at[y, pl.ds(0, NZ - 3), half, quarter]
+            pltpu.make_async_copy(part, part, pz_r.at[0]).wait()
             for o in range(3):
                 push(mine(y), p_s, py_r, {"row": at(0, order[o + 1])}).start()
             px_out(0)
@@ -303,6 +310,7 @@
             px(u, k)
 
     arrived(28 * 64, w_s)
+    part = pt.at[y, pl.ds(0, NZ - 1), half, quarter]
     pltpu.make_async_copy(part, part, pz_s).wait()
     arrived(31 * 64, p_s)
     for sem in (a1_s, a2_s):
@@ -367,7 +375,7 @@
             dma,
             dma,
             dma,
-            dma,
+            dma((3,)),
             dma,
             dma,
             dma((5,)),

time: 49.3 us -> 49.3 us (level)
  the two profiles are of different devices: /device:TPU:8 before, /device:TPU:1 now
where the time goes in v6:
time: 49.3 us; the launch traced here: 49.2 us
  Pallas kernels  49.2 us (100%)
    pallas_call x1, Pallas kernels, shards(): pl.pallas_call(kernel, out_shape=(jax.ShapeDtypeStruct((LOC, FW), BF), ja...  47.6 us
    pallas_call x1, Pallas kernels, shards(): pl.pallas_call(product, out_shape=jax.ShapeDtypeStruct((1, LOC, D), BF),...  1.6 us

profile of v6, /device:TPU:1, one launch (start us, length us, event | category | flops | bytes accessed | tf_op | source)
XLA Modules:
  0.0 49.2 jit_solution(8681303133801740615)
XLA Ops:
  0.0 47.6 %shard_map.73 = (bf16[192,512]{1,0:T(8,128)(2,1)S(1)}, bf16[4,16,32,512]{3,2,1,0:T(8,128)(2,1)S(1)}) custom-call(bf16[1,192,2048]{2,1,0:T(8,128)(2,1)} %tok_hbm.1, bf16[256,512]{1,0:T(8,128)(2,1)} %win_hbm.1, bf16[32,512]{1,0:T(8,128)(2,1)} %bitcast.1, bf16[64,256]{1,0:T(8,128)(2,1)} %constant.8.clone.chan_hbm, ...), custom_call_target="tpu_custom_call" | custom-call | tf_op jit(solution)/shard_map/pallas_call | solution.py:346
  47.6 1.6 %shard_map.74 = bf16[1,192,2048]{2,1,0:T(8,128)(2,1)} custom-call(bf16[192,512]{1,0:T(8,128)(2,1)S(1)} %get-tuple-element.7.lhs_ref, bf16[4,16,32,512]{3,2,1,0:T(8,128)(2,1)S(1)} %get-tuple-element.8.pt_ref), custom_call_target="tpu_custom_call" | custom-call | tf_op jit(solution)/shard_map/pallas_call | solution.py:390

commit v7 on v6

--- a/solution.py
+++ b/solution.py
@@ -118,6 +118,12 @@
         along_x(0, k).start()
     to_mate(0, 0)
 
+    @pl.when(core == 0)
+    def _():
+        for j in range(3):
+            along_x(1, j).start()
+
+
     rid = lax.broadcasted_iota(jnp.int32, (FW, FW), 1)
     fid = lax.broadcasted_iota(jnp.int32, (FW, FW), 0)
     inner = lax.rem(rid, 256)
@@ -171,16 +177,27 @@
         to_mate(0, k + 1)
         along_y(0, k + 1)
         along_y(1, k + 1)
-        if k == 1:
-            for j in range(3):
-                along_x(1, j).start()
+        if k == 2:
             for t in range(1, 4):
                 to_mate(t, 0)
+
+            @pl.when(core == 1)
+            def _():
+                for j in range(3):
+                    along_x(1, j).start()
+
 
     pl.semaphore_wait(hops.at[2], 2)
     tell(3, (at(0, yu), at(0, yd), at(0, yo)))
     own.wait()
     loads[2].wait()
+
+    def pass_x():
+        arrived(192, pin_r.at[3])
+        for k in (1, 2, 3):
+            to_mate(1, k)
+
+    pl.when(core == 0)(pass_x)
     for i in range(2):
         pz_relay(i)
 
@@ -219,9 +236,7 @@
         g = order[t]
         if t == 1:
             pl.semaphore_wait(hops.at[3], 3)
-            arrived(192, pin_r.at[3])
-            for k in (1, 2, 3):
-                to_mate(1, k)
+            pl.when(core == 1)(pass_x)
             arrived(256, yin_r.at[0])
             for k in (1, 2):
                 to_mate(2, k)

time: 49.3 us -> 48.8 us (0.990)
  the two profiles are of different devices: /device:TPU:1 before, /device:TPU:8 now
where the time goes in v7:
time: 48.8 us; the launch traced here: 48.7 us
  Pallas kernels  48.7 us (100%)
    pallas_call x1, Pallas kernels, shards(): pl.pallas_call(kernel, out_shape=(jax.ShapeDtypeStruct((LOC, FW), BF), ja...  47.1 us
    pallas_call x1, Pallas kernels, shards(): pl.pallas_call(product, out_shape=jax.ShapeDtypeStruct((1, LOC, D), BF),...  1.6 us

profile of v7, /device:TPU:8, one launch (start us, length us, event | category | flops | bytes accessed | tf_op | source)
XLA Modules:
  0.0 48.7 jit_solution(815082049232222078)
XLA Ops:
  0.0 47.1 %shard_map.73 = (bf16[192,512]{1,0:T(8,128)(2,1)S(1)}, bf16[4,16,32,512]{3,2,1,0:T(8,128)(2,1)S(1)}) custom-call(bf16[1,192,2048]{2,1,0:T(8,128)(2,1)} %tok_hbm.1, bf16[256,512]{1,0:T(8,128)(2,1)} %win_hbm.1, bf16[32,512]{1,0:T(8,128)(2,1)} %bitcast.1, bf16[64,256]{1,0:T(8,128)(2,1)} %constant.8.clone.chan_hbm, ...), custom_call_target="tpu_custom_call" | custom-call | tf_op jit(solution)/shard_map/pallas_call | solution.py:361
  47.1 1.6 %shard_map.74 = bf16[1,192,2048]{2,1,0:T(8,128)(2,1)} custom-call(bf16[192,512]{1,0:T(8,128)(2,1)S(1)} %get-tuple-element.7.lhs_ref, bf16[4,16,32,512]{3,2,1,0:T(8,128)(2,1)S(1)} %get-tuple-element.8.pt_ref), custom_call_target="tpu_custom_call" | custom-call | tf_op jit(solution)/shard_map/pallas_call | solution.py:405

commit v8 on v7

--- a/solution.py
+++ b/solution.py
@@ -197,9 +197,16 @@
         for k in (1, 2, 3):
             to_mate(1, k)
 
+    def pass_y():
+        arrived(256, yin_r.at[0])
+        for k in (1, 2):
+            to_mate(2, k)
+            to_mate(3, k)
+
     pl.when(core == 0)(pass_x)
     for i in range(2):
         pz_relay(i)
+    pl.when(core == 0)(pass_y)
 
     def far(i):
         step = (i + 1) // 2
@@ -237,10 +244,7 @@
         if t == 1:
             pl.semaphore_wait(hops.at[3], 3)
             pl.when(core == 1)(pass_x)
-            arrived(256, yin_r.at[0])
-            for k in (1, 2):
-                to_mate(2, k)
-                to_mate(3, k)
+            pl.when(core == 1)(pass_y)
         if t == 2:
             arrived(128, yin_r.at[1])
             to_mate(2, 3)

time: 48.8 us -> 49.3 us (1.010)
  the two profiles are of different devices: /device:TPU:8 before, /device:TPU:2 now
where the time goes in v8:
time: 49.3 us; the launch traced here: 49.2 us
  Pallas kernels  49.2 us (100%)
    pallas_call x1, Pallas kernels, shards(): pl.pallas_call(kernel, out_shape=(jax.ShapeDtypeStruct((LOC, FW), BF), ja...  47.6 us
    pallas_call x1, Pallas kernels, shards(): pl.pallas_call(product, out_shape=jax.ShapeDtypeStruct((1, LOC, D), BF),...  1.6 us

profile of v8, /device:TPU:2, one launch (start us, length us, event | category | flops | bytes accessed | tf_op | source)
XLA Modules:
  0.0 49.2 jit_solution(7216989020695287002)
XLA Ops:
  0.0 47.6 %shard_map.73 = (bf16[192,512]{1,0:T(8,128)(2,1)S(1)}, bf16[4,16,32,512]{3,2,1,0:T(8,128)(2,1)S(1)}) custom-call(bf16[1,192,2048]{2,1,0:T(8,128)(2,1)} %tok_hbm.1, bf16[256,512]{1,0:T(8,128)(2,1)} %win_hbm.1, bf16[32,512]{1,0:T(8,128)(2,1)} %bitcast.1, bf16[64,256]{1,0:T(8,128)(2,1)} %constant.8.clone.chan_hbm, ...), custom_call_target="tpu_custom_call" | custom-call | tf_op jit(solution)/shard_map/pallas_call | solution.py:365
  47.6 1.6 %shard_map.74 = bf16[1,192,2048]{2,1,0:T(8,128)(2,1)} custom-call(bf16[192,512]{1,0:T(8,128)(2,1)S(1)} %get-tuple-element.7.lhs_ref, bf16[4,16,32,512]{3,2,1,0:T(8,128)(2,1)S(1)} %get-tuple-element.8.pt_ref), custom_call_target="tpu_custom_call" | custom-call | tf_op jit(solution)/shard_map/pallas_call | solution.py:409
